TPU v7x, 32 devices: a whole 2x2x4 slice. The times are simulated.
32 devices in a mesh: ep: 16 (over z, y, core), tp: 2 (over x).
Axes of the slice: x: 2, y: 2, z: 4, core: 2. Of those that a mesh axis runs over, the one named last changes fastest.
Arguments:
- tokens: bfloat16 [2048, 2048], P('ep'), may hold values from -6 to 6
- expert_ids: int32 [2048, 2], P('ep'), may hold values from 0 to 15, as said below
- route_weights: bfloat16 [2048, 2], P('ep'), may hold values from 0.099609375 to 1
- cotangent: bfloat16 [2048, 2048], P('ep'), may hold values from -3 to 3
- w_gate: bfloat16 [16, 2048, 512], P('ep', None, 'tp'), may hold values from -0.125 to 0.125
- w_up: bfloat16 [16, 2048, 512], P('ep', None, 'tp'), may hold values from -0.125 to 0.125
- w_down: bfloat16 [16, 512, 2048], P('ep', 'tp'), may hold values from -0.25 to 0.25
Outputs:
- token_grad: bfloat16 [2048, 2048], P('ep', 'tp')
- route_grad: bfloat16 [2048, 2], P('ep')
- grad_gate: bfloat16 [16, 2048, 512], P('ep', None, 'tp')
- grad_up: bfloat16 [16, 2048, 512], P('ep', None, 'tp')
- grad_down: bfloat16 [16, 512, 2048], P('ep', 'tp')
- gate_rows: float32 [16, 2048], P('ep')
- up_rows: float32 [16, 2048], P('ep')
- down_rows: float32 [16, 512], P('ep', 'tp')
Inputs may be any that keep to these rules, and one draw needn't show every extreme that they name: `expert_ids`: each row names 2 different experts of one group: both lie in g * 4 to (g + 1) * 4 - 1 for the row's group g. In the rows of one device (aligned blocks of 128 rows) no expert is named more than 32 times, and in every block some expert is named exactly 32 times.
All inputs are finite; a program needn't handle non-finite values.
Results may differ from a plain program's by a relative error of at most 0.012.
Values may be sent and summed in bfloat16 or wider, within the bound.
A program may use at most 64 MiB of HBM per device.

v0:
```python
import jax
import jax.numpy as jnp
from jax import lax
from jax.sharding import PartitionSpec as P

TOPK = 2


def on_device(tokens, expert_ids, route_weights, cotangent, w_gate, w_up, w_down):
    tok_rows, model_width = tokens.shape
    experts = lax.axis_size("ep")
    splits = lax.axis_size("tp")
    capacity = 2 * tok_rows * TOPK // experts
    slot_count = experts * capacity
    assigns = tok_rows * TOPK
    flat_ids = expert_ids.reshape(-1)
    onehot = (flat_ids[:, None] == jnp.arange(experts, dtype=jnp.int32)[None, :]).astype(
        jnp.float32
    )
    assign_order = jnp.arange(assigns, dtype=jnp.int32)
    earlier = (assign_order[:, None] > assign_order[None, :]).astype(jnp.float32)
    before = jnp.dot(earlier, onehot, precision=lax.Precision.HIGHEST)
    slot_rank = jnp.sum(before * onehot, axis=1).astype(jnp.int32)
    position = flat_ids * capacity + slot_rank
    slot_owner = jnp.full((slot_count,), tok_rows, jnp.int32).at[position].set(assign_order // TOPK)
    slot_scale = jnp.zeros((slot_count,), jnp.bfloat16).at[position].set(route_weights.reshape(-1))
    slice_width = model_width // splits
    slice_start = lax.axis_index("tp") * slice_width
    rows_slice = lax.dynamic_slice_in_dim(tokens, slice_start, slice_width, 1)
    cot_slice = lax.dynamic_slice_in_dim(cotangent, slice_start, slice_width, 1)
    rows_pad = jnp.concatenate([rows_slice, jnp.zeros((1, slice_width), jnp.bfloat16)], axis=0)
    cot_pad = jnp.concatenate([cot_slice, jnp.zeros((1, slice_width), jnp.bfloat16)], axis=0)
    outgoing = rows_pad[slot_owner]
    outgoing_cot = cot_pad[slot_owner]
    part_rows, part_cot, got_scale = (
        lax.all_to_all(outgoing, "ep", split_axis=0, concat_axis=0, tiled=True),
        lax.all_to_all(outgoing_cot, "ep", split_axis=0, concat_axis=0, tiled=True),
        lax.all_to_all(slot_scale, "ep", split_axis=0, concat_axis=0, tiled=True),
    )
    slot_rows, slot_cot = (
        lax.all_gather(part_rows, "tp", axis=1, tiled=True),
        lax.all_gather(part_cot, "tp", axis=1, tiled=True),
    )
    scale_col = got_scale.reshape(slot_count, 1).astype(jnp.float32)
    gate_cols = w_gate[0]
    up_cols = w_up[0]
    down_part = w_down[0]
    gate_pre = jnp.dot(slot_rows, gate_cols, preferred_element_type=jnp.float32)
    up_pre = jnp.dot(slot_rows, up_cols, preferred_element_type=jnp.float32)
    hidden_back = lax.dot_general(
        slot_cot, down_part, (((1,), (1,)), ((), ())), preferred_element_type=jnp.float32
    )
    gate_sig = jax.nn.sigmoid(gate_pre)
    activated = gate_pre * gate_sig
    hidden = activated * up_pre
    route_part = jnp.sum(hidden * hidden_back, axis=1)
    hidden_cot = scale_col * hidden_back
    up_cot = (hidden_cot * activated).astype(jnp.bfloat16)
    gate_cot = (hidden_cot * up_pre * gate_sig * (1.0 + gate_pre * (1.0 - gate_sig))).astype(
        jnp.bfloat16
    )
    weighted_hidden = (scale_col * hidden).astype(jnp.bfloat16)
    grad_down = lax.dot_general(
        weighted_hidden, slot_cot, (((0,), (0,)), ((), ())), preferred_element_type=jnp.float32
    ).astype(jnp.bfloat16)
    grad_gate = lax.dot_general(
        slot_rows, gate_cot, (((0,), (0,)), ((), ())), preferred_element_type=jnp.float32
    ).astype(jnp.bfloat16)
    grad_up = lax.dot_general(
        slot_rows, up_cot, (((0,), (0,)), ((), ())), preferred_element_type=jnp.float32
    ).astype(jnp.bfloat16)
    token_term = lax.dot_general(
        gate_cot, gate_cols, (((1,), (1,)), ((), ())), preferred_element_type=jnp.float32
    )
    token_term = token_term + lax.dot_general(
        up_cot, up_cols, (((1,), (1,)), ((), ())), preferred_element_type=jnp.float32
    )
    reduced = lax.psum_scatter(
        token_term.astype(jnp.bfloat16), "tp", scatter_dimension=1, tiled=True
    )
    gate_square = jnp.sum(jnp.square(grad_gate.astype(jnp.float32)), axis=1)
    up_square = jnp.sum(jnp.square(grad_up.astype(jnp.float32)), axis=1)
    down_square = jnp.sum(jnp.square(grad_down.astype(jnp.float32)), axis=1)
    route_total, gate_rows, up_rows = lax.psum((route_part, gate_square, up_square), "tp")
    back_rows, back_route = (
        lax.all_to_all(reduced, "ep", split_axis=0, concat_axis=0, tiled=True),
        lax.all_to_all(
            route_total.astype(jnp.bfloat16), "ep", split_axis=0, concat_axis=0, tiled=True
        ),
    )
    per_assign = back_rows[position].astype(jnp.float32).reshape(tok_rows, TOPK, -1)
    token_grad = jnp.sum(per_assign, axis=1).astype(jnp.bfloat16)
    route_grad = back_route[position].reshape(tok_rows, TOPK)
    return (
        token_grad,
        route_grad,
        grad_gate[None],
        grad_up[None],
        grad_down[None],
        gate_rows[None],
        up_rows[None],
        down_square[None],
    )


def solution(mesh):
    return jax.shard_map(
        on_device,
        mesh=mesh,
        in_specs=(
            P("ep", None),
            P("ep", None),
            P("ep", None),
            P("ep", None),
            P("ep", None, "tp"),
            P("ep", None, "tp"),
            P("ep", "tp", None),
        ),
        out_specs=(
            P("ep", "tp"),
            P("ep", None),
            P("ep", None, "tp"),
            P("ep", None, "tp"),
            P("ep", "tp", None),
            P("ep", None),
            P("ep", None),
            P("ep", "tp"),
        ),
        check_vma=False,
    )
```

profile of v0, /device:TPU:0, one launch (start us, length us, event | category | flops | bytes accessed | tf_op | source)
XLA Modules:
  0.0 191.2 jit_solution(12211207150902373876)
XLA Ops:
  9.4 1.4 scatter_custom_fusion.1
  11.9 2.1 %gather_fusion.1 = bf16[512,1024]{1,0:T(8,128)(2,1)S(1)} fusion(bf16[129,1024]{1,0:T(8,128)(2,1)S(1)} %concatenate.7, s32[1024]{0:T(1024)S(1)} %pad_clamp_fusion.1), kind=kCustom, calls=%fused_computation.1 | custom fusion | bytes 2099200 | tf_op jit(solution)/shard_map/gather | solution.py:33
  14.0 32.0 %all_to_all.59 = bf16[16,32,1024]{2,1,0:T(8,128)(2,1)} all-to-all(bf16[16,32,1024]{2,1,0:T(8,128)(2,1)S(1)} %bitcast.43), channel_id=1, replica_groups=mesh['ep'=16,'tp'=2] {'ep'}, dimensions={0} | all-to-all | bytes 2097152 | tf_op jit(solution)/shard_map/all_to_all | solution.py:36
  46.1 2.1 %gather_fusion = bf16[512,1024]{1,0:T(8,128)(2,1)S(1)} fusion(bf16[129,1024]{1,0:T(8,128)(2,1)S(1)} %concatenate.6, s32[1024]{0:T(1024)S(1)} %pad_clamp_fusion.1), kind=kCustom, calls=%fused_computation | custom fusion | bytes 2099200 | tf_op jit(solution)/shard_map/gather | solution.py:34
  48.2 29.6 %all_to_all.60 = bf16[16,32,1024]{2,1,0:T(8,128)(2,1)} all-to-all(bf16[16,32,1024]{2,1,0:T(8,128)(2,1)S(1)} %bitcast.42), channel_id=1, replica_groups=mesh['ep'=16,'tp'=2] {'ep'}, dimensions={0} | all-to-all | bytes 2097152 | tf_op jit(solution)/shard_map/all_to_all | solution.py:37
  78.2 2.2 %scatter_custom_fusion = bf16[512]{0:T(512)(128)(2,1)S(1)} fusion(s32[256]{0:T(256)S(1)} %bitcast.52, bf16[256]{0:T(256)(128)(2,1)S(1)} %reshape.116, bf16[]{:T(256)} %constant.13.clone.1), kind=kCustom, calls=%fused_computation.49 | custom fusion | bytes 1026 | tf_op jit(solution)/shard_map/scatter | solution.py:26
  80.5 11.3 %all_to_all.61 = bf16[16,32,1]{1,2,0:T(2,128)(2,1)S(1)} all-to-all(bf16[16,32,1]{1,2,0:T(2,128)(2,1)S(1)} %all_to_all.52), channel_id=1, replica_groups=mesh['ep'=16,'tp'=2] {'ep'}, dimensions={0} | all-to-all | bytes 2048 | tf_op jit(solution)/shard_map/all_to_all | solution.py:38
  91.8 2.5 %fusion.3 = f32[512,256]{0,1:T(8,128)S(1)} fusion(bf16[512,2048]{1,0:T(8,128)(2,1)} %all-gather.5.cloned.1.call-done, bf16[1,2048,256]{2,1,0:T(8,128)(2,1)S(1)} %copy-done), kind=kOutput, calls=%fused_computation.17 | convolution fusion | flops 536870912 | bytes 3670016 | tf_op jit(solution)/shard_map/dot_general | solution.py:48
  94.3 1.6 fusion.6
  95.9 18.4 %all-gather.3.cloned.1.call-done = bf16[512,2048]{1,0:T(8,128)(2,1)} async-done(((bf16[512,1024]{1,0:T(8,128)(2,1)}), bf16[512,2048]{1,0:T(8,128)(2,1)}) %all-gather.3.cloned.1.call-update) | async-done | bytes 2097168 | tf_op jit(solution)/shard_map/all_gather | solution.py:42
  114.3 2.9 %multiply_reduce_fusion.3 = (f32[512]{0:T(512)S(1)}, bf16[512,256]{0,1:T(8,128)(2,1)S(1)}, bf16[512,256]{0,1:T(8,128)(2,1)S(1)}) fusion(f32[512,256]{0,1:T(8,128)} %fusion.6, f32[512,256]{0,1:T(8,128)S(1)} %fusion.3, f32[512]{0:T(512)S(1)} %reshape.79, bf16[512,2048]{1,0:T(8,128)(2,1)} %all-gather.3.cloned.1.call-done, bf16[1,256,2048]{2,1,0:T(8,128)(2,1)} %param.13), kind=kOutput, calls=%fused_computation.25 | convolution fusion | flops 539098624 | bytes 4722688 | tf_op jit(solution)/shard_map/dot_general | solution.py:50
  118.0 2.1 %add_convert_fusion = bf16[512,2048]{1,0:T(8,128)(2,1)} fusion(f32[512,2048]{1,0:T(8,128)S(1)} %fusion.1, bf16[512,256]{0,1:T(8,128)(2,1)S(1)} %get-tuple-element.37, bf16[1,2048,256]{2,1,0:T(8,128)(2,1)S(1)} %copy-done.1), kind=kOutput, calls=%fused_computation.6 | convolution fusion | flops 538968064 | bytes 7602176 | tf_op jit(solution)/shard_map/dot_general | solution.py:75
  120.2 2.5 %multiply_reduce_fusion.2 = (f32[2048]{0:T(1024)S(1)}, bf16[2048,256]{0,1:T(8,128)(2,1)S(1)}) fusion(bf16[512,256]{0,1:T(8,128)(2,1)S(1)} %get-tuple-element.36, bf16[512,2048]{1,0:T(8,128)(2,1)} %all-gather.5.cloned.1.call-done), kind=kOutput, calls=%fused_computation.12 | convolution fusion | flops 538966016 | bytes 3416064 | tf_op jit(solution)/shard_map/dot_general | solution.py:66
  122.7 1.7 multiply_reduce_fusion.1
  124.4 8.3 %all-reduce.2 = (bf16[512]{0:T(512)(128)(2,1)S(1)}, f32[1,2048]{1,0:T(1,128)}, f32[1,2048]{1,0:T(1,128)}) all-reduce(f32[512]{0:T(512)S(1)} %get-tuple-element.35, f32[1,2048]{1,0:T(1,128)S(1)} %bitcast.49, f32[1,2048]{1,0:T(1,128)S(1)} %bitcast.50), channel_id=1, replica_groups=mesh['ep'=16,'tp'=2] {'tp'}, use_global_device_ids=true, to_apply=%region_6.7 | all-reduce | flops 4608 | bytes 35840 | tf_op jit(solution)/shard_map/psum | solution.py:84
  132.8 12.0 %all_to_all.62 = bf16[16,32,1]{1,2,0:T(2,128)(2,1)S(1)} all-to-all(bf16[16,32,1]{1,2,0:T(2,128)(2,1)S(1)} %all_to_all.53), channel_id=1, replica_groups=mesh['ep'=16,'tp'=2] {'ep'}, dimensions={0} | all-to-all | bytes 2048 | tf_op jit(solution)/shard_map/all_to_all | solution.py:87
  144.8 7.9 %reduce-scatter.2.cloned.1.call-done = bf16[512,1024]{1,0:T(8,128)(2,1)} async-done(((bf16[512,2048]{1,0:T(8,128)(2,1)}), bf16[512,1024]{1,0:T(8,128)(2,1)}) %reduce-scatter.2.cloned.1.call-update) | async-done | bytes 1048592 | tf_op jit(solution)/shard_map/reduce_scatter | solution.py:78
  152.7 5.6 %all-to-all-start.3 = ((bf16[16,32,1024]{2,1,0:T(8,128)(2,1)}), bf16[16,32,1024]{2,1,0:T(8,128)(2,1)S(1)}, u32[]{:S(2)}, u32[]{:S(2)}) async-start(bf16[16,32,1024]{2,1,0:T(8,128)(2,1)} %bitcast.46), calls=%async_computation.4 | async-start | bytes 2097152 | tf_op jit(solution)/shard_map/all_to_all | solution.py:86
  158.3 2.3 %copy.30 = bf16[1,2048,256]{2,1,0:T(8,128)(2,1)} copy(bf16[1,2048,256]{1,2,0:T(8,128)(2,1)} %bitcast.48) | data formatting | bytes 2097152
  160.6 1.3 copy.29
  161.9 4.2 %multiply_reduce_fusion = (f32[256]{0:T(256)}, bf16[256,2048]{1,0:T(8,128)(2,1)}) fusion(bf16[512,2048]{1,0:T(8,128)(2,1)} %all-gather.3.cloned.1.call-done, f32[512]{0:T(512)S(1)} %reshape.79, f32[512,256]{0,1:T(8,128)} %fusion.6, f32[512,256]{0,1:T(8,128)} %copy-done.5), kind=kOutput, calls=%fused_computation.10 | convolution fusion | flops 539885312 | bytes 4197376 | tf_op jit(solution)/shard_map/dot_general | solution.py:63
  166.2 1.9 %gather_fusion.3 = bf16[256]{0:T(256)(128)(2,1)S(1)} fusion(bf16[512]{0:T(512)(128)(2,1)S(1)} %all_to_all.51, s32[1024]{0:T(1024)S(1)} %pad_clamp_fusion), kind=kCustom, calls=%fused_computation.3 | custom fusion | bytes 2048 | tf_op jit(solution)/shard_map/gather | solution.py:93
  168.9 12.3 %all-to-all-done.3 = bf16[16,32,1024]{2,1,0:T(8,128)(2,1)S(1)} async-done(((bf16[16,32,1024]{2,1,0:T(8,128)(2,1)}), bf16[16,32,1024]{2,1,0:T(8,128)(2,1)S(1)}, u32[]{:S(2)}, u32[]{:S(2)}) %all-to-all-start.3) | async-done | bytes 1048608 | tf_op jit(solution)/shard_map/all_to_all | solution.py:86
  182.6 2.1 %reduce_sum.58 = bf16[128,1024]{1,0:T(8,128)(2,1)} reduce(bf16[128,2,1024]{2,1,0:T(2,128)(2,1)S(1)} %gather.17, bf16[]{:T(256)} %constant.13.clone.1), dimensions={1}, to_apply=%region_4.5 | reduce | flops 131072 | bytes 786434 | tf_op jit(solution)/shard_map/reduce_sum | solution.py:92
  (47 shorter events, 7.1 us)
Async XLA Ops:
  7.2 84.6 %copy-start = (bf16[1,2048,256]{2,1,0:T(8,128)(2,1)S(1)}, bf16[1,2048,256]{2,1,0:T(8,128)(2,1)}, u32[]{:S(2)}) copy-start(bf16[1,2048,256]{2,1,0:T(8,128)(2,1)} %param.11) | copy-start | bytes 3145732
  7.2 84.6 %all-gather.5.cloned.1.call-start = ((), (), s32[]{:S(2)}) async-start(), calls=%async_computation.7 | async-start | bytes 3145728 | tf_op jit(solution)/shard_map/all_gather | solution.py:41
  46.0 68.3 %all-gather.3.cloned.1.call-start = ((), (), s32[]{:S(2)}) async-start(), calls=%async_computation.6 | async-start | bytes 3145728 | tf_op jit(solution)/shard_map/all_gather | solution.py:42
  48.2 29.7 %copy-start.2 = (bf16[128,2]{0,1:T(2,128)(2,1)S(1)}, bf16[128,2]{0,1:T(2,128)(2,1)}, u32[]{:S(2)}) copy-start(bf16[128,2]{0,1:T(2,128)(2,1)} %param.9) | copy-start | bytes 1540
  77.8 16.5 %copy-start.1 = (bf16[1,2048,256]{2,1,0:T(8,128)(2,1)S(1)}, bf16[1,2048,256]{2,1,0:T(8,128)(2,1)}, u32[]{:S(2)}) copy-start(bf16[1,2048,256]{2,1,0:T(8,128)(2,1)} %param.12) | copy-start | bytes 3145732
  77.8 74.8 %reduce-scatter.2.cloned.1.call-start = ((), (), s32[]{:S(2)}) async-start(), calls=%async_computation.8 | async-start | bytes 3145728 | tf_op jit(solution)/shard_map/reduce_scatter | solution.py:78
  91.8 2.5 %copy-start.3 = (bf16[512,2048]{1,0:T(8,128)(2,1)S(1)}, bf16[512,2048]{1,0:T(8,128)(2,1)}, u32[]{:S(2)}) copy-start(bf16[512,2048]{1,0:T(8,128)(2,1)} %all-gather.5.cloned.1.call-done) | copy-start | bytes 6291460
  94.3 22.9 %copy-start.5 = (f32[512,256]{0,1:T(8,128)}, f32[512,256]{0,1:T(8,128)S(1)}, u32[]{:S(2)}) copy-start(f32[512,256]{0,1:T(8,128)S(1)} %fusion.3) | copy-start | bytes 1572868
  120.2 2.5 %copy-start.4 = (bf16[512,2048]{1,0:T(8,128)(2,1)S(1)}, bf16[512,2048]{1,0:T(8,128)(2,1)}, u32[]{:S(2)}) copy-start(bf16[512,2048]{1,0:T(8,128)(2,1)} %all-gather.5.cloned.1.call-done) | copy-start | bytes 6291460
  152.7 28.5 %all-to-all-start.3 = ((bf16[16,32,1024]{2,1,0:T(8,128)(2,1)}), bf16[16,32,1024]{2,1,0:T(8,128)(2,1)S(1)}, u32[]{:S(2)}, u32[]{:S(2)}) async-start(bf16[16,32,1024]{2,1,0:T(8,128)(2,1)} %bitcast.46), calls=%async_computation.4 | async-start | bytes 2097152 | tf_op jit(solution)/shard_map/all_to_all | solution.py:86
Sparse Core Ops, SparseCore 0:
  46.2 33.4 all-gather.4
  81.2 33.0 all-gather.2
  120.3 32.2 reduce-scatter.1
where the time goes:
time: 193 us; the launch traced here: 191 us
  blocking collectives  93.2 us (48%)
  waiting for transfers between devices  38.6 us (20%)
  matrix products  18.5 us (10%)
  local copies, waits for them, and re-layouts  18.2 us (9%)
  between operations  14 us (7%)
  starting transfers between devices  5.75 us (3%)
  other arithmetic  3 us (2%)
    all_to_all x1, blocking collectives, on_device(): lax.all_to_all(outgoing, 'ep', split_axis=0, concat_axis=0, tiled=True)  32 us
    all_to_all x1, blocking collectives, on_device(): lax.all_to_all(outgoing_cot, 'ep', split_axis=0, concat_axis=0, tiled=True)  29.6 us
    all_gather x1, waiting for transfers between devices, on_device(): lax.all_gather(part_cot, 'tp', axis=1, tiled=True)  18.4 us
    all_to_all x1, waiting for transfers between devices, on_device(): lax.all_to_all(reduced, 'ep', split_axis=0, concat_axis=0, tiled=True)  12.3 us
    all_to_all x1, blocking collectives, on_device(): lax.all_to_all(route_total.astype(jnp.bfloat16), 'ep', split_axis=0, conc...  12 us
    all_to_all x1, blocking collectives, on_device(): lax.all_to_all(slot_scale, 'ep', split_axis=0, concat_axis=0, tiled=True)  11.3 us
    psum x1, blocking collectives, on_device(): lax.psum((route_part, gate_square, up_square), 'tp')  8.27 us
    reduce_scatter x1, waiting for transfers between devices, on_device(): lax.psum_scatter(token_term.astype(jnp.bfloat16), 'tp', scatter_dimension...  7.87 us
  transfers between devices with their start and end apart: 4, of which 3 were waited for; matrix products, arithmetic and copies ran while one was open for 12% of the time, Pallas kernels for 0%

commit v1 on v0

v1 whole, which is shorter than its diff:
```python
import functools

import jax
import jax.numpy as jnp
from jax import lax
from jax.experimental import pallas as pl
from jax.experimental.pallas import tpu as pltpu
from jax.sharding import PartitionSpec as P

MESH = pl.DeviceIdType.MESH
LANES = 128


def greet(experts, splits, me, col):
    barrier = pltpu.get_barrier_semaphore()

    @pl.loop(1, experts)
    def _(off):
        pl.semaphore_signal(
            barrier, inc=1, device_id={"ep": lax.rem(me + off, experts), "tp": col}, device_id_type=MESH
        )

    for shift in range(1, splits):
        pl.semaphore_signal(
            barrier, inc=1, device_id={"ep": me, "tp": lax.rem(col + shift, splits)}, device_id_type=MESH
        )
    pl.semaphore_wait(barrier, experts - 1 + splits - 1)


def remote(src, dst, send, recv, ep, tp):
    return pltpu.make_async_remote_copy(
        src_ref=src,
        dst_ref=dst,
        send_sem=send,
        recv_sem=recv,
        device_id={"ep": ep, "tp": tp},
        device_id_type=MESH,
    )


def dispatch_kernel(
    experts, splits, rows_ref, cot_ref, scale_ref, rows_out, cot_out, scale_out,
    send, recv, relay_send, relay_recv, local,
):
    me = lax.axis_index("ep")
    col = lax.axis_index("tp")
    width = rows_ref.shape[2]
    mine = pl.ds(pl.multiple_of(col * width, LANES), width)
    greet(experts, splits, me, col)
    pairs = ((rows_ref, rows_out), (cot_ref, cot_out))

    def out_copies(off):
        there = lax.rem(me + off, experts)
        copies = [
            remote(src.at[there], dst.at[me, :, mine], send.at[i, off], recv.at[i, off], there, col)
            for i, (src, dst) in enumerate(pairs)
        ]
        copies.append(
            remote(scale_ref.at[there], scale_out.at[me], send.at[2, off], recv.at[2, off], there, col)
        )
        return copies

    def relays(off, shift, i):
        source = lax.rem(me + experts - off, experts)
        block = pairs[i][1].at[source, :, mine]
        peer = lax.rem(col + shift, splits)
        return remote(block, block, relay_send.at[i, shift - 1, off], relay_recv.at[i, shift - 1, off], me, peer)

    own = [
        pltpu.make_async_copy(src.at[me], dst.at[me, :, mine], local.at[i])
        for i, (src, dst) in enumerate(pairs)
    ]
    own.append(pltpu.make_async_copy(scale_ref.at[me], scale_out.at[me], local.at[2]))
    for copy in own:
        copy.start()

    @pl.loop(1, experts)
    def _(off):
        for copy in out_copies(off):
            copy.start()

    for copy in own:
        copy.wait()
    for shift in range(1, splits):
        for i in range(2):
            relays(0, shift, i).start()

    @pl.loop(1, experts)
    def _(off):
        copies = out_copies(off)
        for i in range(2):
            copies[i].wait_recv()
            for shift in range(1, splits):
                relays(off, shift, i).start()

    @pl.loop(1, experts)
    def _(off):
        copies = out_copies(off)
        for copy in copies:
            copy.wait_send()
        copies[2].wait_recv()

    @pl.loop(0, experts)
    def _(off):
        for shift in range(1, splits):
            for i in range(2):
                relays(off, shift, i).wait_send()
                source = lax.rem(me + experts - off, experts)
                peer = lax.rem(col + splits - shift, splits)
                part = pl.ds(pl.multiple_of(peer * width, LANES), width)
                block = pairs[i][1].at[source, :, part]
                remote(
                    block, block, relay_send.at[i, shift - 1, off], relay_recv.at[i, shift - 1, off], me, peer
                ).wait_recv()


def dispatch(rows, cot, scale, experts, splits):
    capacity, width = rows.shape[1:]
    whole = jax.ShapeDtypeStruct((experts, capacity, width * splits), jnp.bfloat16)
    vmem = pl.BlockSpec(memory_space=pltpu.VMEM)
    return pl.pallas_call(
        functools.partial(dispatch_kernel, experts, splits),
        out_shape=(whole, whole, jax.ShapeDtypeStruct(scale.shape, scale.dtype)),
        in_specs=[vmem] * 3,
        out_specs=(vmem,) * 3,
        scratch_shapes=[
            pltpu.SemaphoreType.DMA((3, experts)),
            pltpu.SemaphoreType.DMA((3, experts)),
            pltpu.SemaphoreType.DMA((2, splits - 1, experts)),
            pltpu.SemaphoreType.DMA((2, splits - 1, experts)),
            pltpu.SemaphoreType.DMA((3,)),
        ],
        compiler_params=pltpu.CompilerParams(collective_id=0, has_side_effects=True),
    )(rows, cot, scale)


def combine_kernel(
    experts, splits, part_ref, route_ref, square_ref, back, back_route, square_out,
    peer_part, total, peer_route, route_total,
    swap_send, swap_recv, small_send, small_recv, send, recv,
):
    me = lax.axis_index("ep")
    col = lax.axis_index("tp")
    width = back.shape[2]
    mine = pl.ds(pl.multiple_of(col * width, LANES), width)
    greet(experts, splits, me, col)

    def swap(off, shift):
        source = lax.rem(me + off, experts)
        peer = lax.rem(col + shift, splits)
        theirs = pl.ds(pl.multiple_of(peer * width, LANES), width)
        return remote(
            part_ref.at[source, :, theirs], peer_part.at[shift - 1, source],
            swap_send.at[shift - 1, off], swap_recv.at[shift - 1, off], me, peer,
        )

    small = []
    for shift in range(1, splits):
        peer = lax.rem(col + shift, splits)
        small.append((
            remote(route_ref, peer_route.at[shift - 1], small_send.at[0, shift - 1],
                   small_recv.at[0, shift - 1], me, peer),
            remote(square_ref, square_out.at[shift - 1], small_send.at[1, shift - 1],
                   small_recv.at[1, shift - 1], me, peer),
        ))
    for shift in range(1, splits):
        small[shift - 1][0].start()

    @pl.loop(1, experts + 1)
    def _(step):
        for shift in range(1, splits):
            swap(lax.rem(step, experts), shift).start()

    for shift in range(1, splits):
        small[shift - 1][1].start()

    def block_total(off):
        source = lax.rem(me + off, experts)
        for shift in range(1, splits):
            swap(off, shift).wait_recv()
        value = part_ref[source, :, mine].astype(jnp.float32)
        for shift in range(1, splits):
            value = value + peer_part[shift - 1, source].astype(jnp.float32)
        return value.astype(back.dtype)

    def out_copies(off):
        there = lax.rem(me + off, experts)
        return (
            remote(total.at[there], back.at[me], send.at[0, off], recv.at[0, off], there, col),
            remote(route_total.at[there], back_route.at[me], send.at[1, off], recv.at[1, off], there, col),
        )

    value = route_ref[...]
    for shift in range(1, splits):
        small[shift - 1][0].wait_recv()
        value = value + peer_route[shift - 1]
    route_total[...] = value
    back_route[me] = route_total[me]

    @pl.loop(1, experts)
    def _(off):
        total[lax.rem(me + off, experts)] = block_total(off)
        for copy in out_copies(off):
            copy.start()

    back[me] = block_total(0)

    @pl.loop(1, experts)
    def _(off):
        for copy in out_copies(off):
            copy.wait()

    @pl.loop(0, experts)
    def _(off):
        for shift in range(1, splits):
            swap(off, shift).wait_send()

    for shift in range(1, splits):
        small[shift - 1][0].wait_send()
        small[shift - 1][1].wait()


def combine(part, route, squares, experts, splits):
    capacity, model_width = part.shape[1:]
    width = model_width // splits
    vmem = pl.BlockSpec(memory_space=pltpu.VMEM)
    return pl.pallas_call(
        functools.partial(combine_kernel, experts, splits),
        out_shape=(
            jax.ShapeDtypeStruct((experts, capacity, width), jnp.bfloat16),
            jax.ShapeDtypeStruct(route.shape, jnp.float32),
            jax.ShapeDtypeStruct((splits - 1,) + squares.shape, jnp.float32),
        ),
        in_specs=[vmem] * 3,
        out_specs=(vmem,) * 3,
        scratch_shapes=[
            pltpu.VMEM((splits - 1, experts, capacity, width), jnp.bfloat16),
            pltpu.VMEM((experts, capacity, width), jnp.bfloat16),
            pltpu.VMEM((splits - 1,) + route.shape, jnp.float32),
            pltpu.VMEM(route.shape, jnp.float32),
            pltpu.SemaphoreType.DMA((splits - 1, experts)),
            pltpu.SemaphoreType.DMA((splits - 1, experts)),
            pltpu.SemaphoreType.DMA((2, splits - 1)),
            pltpu.SemaphoreType.DMA((2, splits - 1)),
            pltpu.SemaphoreType.DMA((2, experts)),
            pltpu.SemaphoreType.DMA((2, experts)),
        ],
        compiler_params=pltpu.CompilerParams(collective_id=1, has_side_effects=True),
    )(part, route, squares)


def on_device(tokens, expert_ids, route_weights, cotangent, w_gate, w_up, w_down):
    tok_rows, model_width = tokens.shape
    topk = expert_ids.shape[1]
    experts = lax.axis_size("ep")
    splits = lax.axis_size("tp")
    capacity = 2 * tok_rows * topk // experts
    slot_count = experts * capacity
    f32, bf16 = jnp.float32, jnp.bfloat16

    expert_iota = jnp.arange(experts, dtype=jnp.int32)[None, :]
    slots = jnp.arange(slot_count, dtype=jnp.int32)[None, :]
    slot_expert = slots // capacity
    spread = (expert_iota.reshape(experts, 1) == slot_expert).astype(bf16)
    picks = [expert_ids[:, k : k + 1] == expert_iota for k in range(topk)]
    member = sum(p.astype(f32) for p in picks)
    weight = sum(
        jnp.where(p, route_weights[:, k : k + 1].astype(f32), 0.0) for k, p in enumerate(picks)
    ).astype(bf16)
    order = jnp.arange(tok_rows, dtype=jnp.int32)
    earlier = (order[:, None] > order[None, :]).astype(bf16)
    before = jnp.dot(earlier, member.astype(bf16), preferred_element_type=f32)
    rank = jnp.where(member > 0, before, -1.0).astype(bf16)
    slot_rank = jnp.dot(rank, spread, preferred_element_type=f32)
    chosen = slot_rank == (slots % capacity).astype(f32)
    select = chosen.astype(bf16)
    slot_weight = jnp.sum(
        jnp.where(chosen, jnp.dot(weight, spread, preferred_element_type=f32), 0.0), axis=0
    )
    width = model_width // splits
    start = lax.axis_index("tp") * width

    def pack(array):
        piece = lax.dynamic_slice_in_dim(array, start, width, 1)
        packed = lax.dot_general(select, piece, (((0,), (0,)), ((), ())), preferred_element_type=f32)
        return packed.astype(bf16).reshape(experts, capacity, width)

    lane_pad = -capacity % LANES
    scale_out = jnp.pad(slot_weight.reshape(experts, 1, capacity), ((0, 0), (0, 0), (0, lane_pad)))
    slot_rows, slot_cot, got_scale = dispatch(
        pack(tokens), pack(cotangent), scale_out, experts, splits
    )
    slot_rows = slot_rows.reshape(slot_count, model_width)
    slot_cot = slot_cot.reshape(slot_count, model_width)
    scale_col = got_scale[:, 0, :capacity].reshape(slot_count, 1)

    gate_cols = w_gate[0]
    up_cols = w_up[0]
    down_part = w_down[0]
    gate_pre = jnp.dot(slot_rows, gate_cols, preferred_element_type=f32)
    up_pre = jnp.dot(slot_rows, up_cols, preferred_element_type=f32)
    hidden_back = lax.dot_general(
        slot_cot, down_part, (((1,), (1,)), ((), ())), preferred_element_type=f32
    )
    gate_sig = jax.nn.sigmoid(gate_pre)
    activated = gate_pre * gate_sig
    hidden = activated * up_pre
    route_part = jnp.sum(hidden * hidden_back, axis=1)
    hidden_cot = scale_col * hidden_back
    up_cot = (hidden_cot * activated).astype(bf16)
    gate_cot = (hidden_cot * up_pre * gate_sig * (1.0 + gate_pre * (1.0 - gate_sig))).astype(bf16)
    weighted_hidden = (scale_col * hidden).astype(bf16)

    def outer(left, right):
        return lax.dot_general(
            left, right, (((0,), (0,)), ((), ())), preferred_element_type=f32
        ).astype(bf16)

    grad_down = outer(weighted_hidden, slot_cot)
    grad_gate = outer(slot_rows, gate_cot)
    grad_up = outer(slot_rows, up_cot)
    token_term = lax.dot_general(
        gate_cot, gate_cols, (((1,), (1,)), ((), ())), preferred_element_type=f32
    )
    token_term = token_term + lax.dot_general(
        up_cot, up_cols, (((1,), (1,)), ((), ())), preferred_element_type=f32
    )
    gate_square = jnp.sum(jnp.square(grad_gate.astype(f32)), axis=1)
    up_square = jnp.sum(jnp.square(grad_up.astype(f32)), axis=1)
    down_square = jnp.sum(jnp.square(grad_down.astype(f32)), axis=1)
    squares = jnp.stack([gate_square, up_square])
    route_out = jnp.pad(route_part.reshape(experts, 1, capacity), ((0, 0), (0, 0), (0, lane_pad)))
    back_rows, back_route, peer_squares = combine(
        token_term.astype(bf16).reshape(experts, capacity, model_width),
        route_out, squares, experts, splits,
    )
    squares = squares + jnp.sum(peer_squares, axis=0)
    token_grad = jnp.dot(
        select, back_rows.reshape(slot_count, width), preferred_element_type=f32
    ).astype(bf16)
    slot_route = back_route[:, 0, :capacity].reshape(1, slot_count)
    route_grad = jnp.concatenate(
        [
            jnp.sum(
                jnp.where(chosen & (slot_expert == expert_ids[:, k : k + 1]), slot_route, 0.0),
                axis=1, keepdims=True,
            )
            for k in range(topk)
        ],
        axis=1,
    ).astype(bf16)
    return (
        token_grad,
        route_grad,
        grad_gate[None],
        grad_up[None],
        grad_down[None],
        squares[0:1],
        squares[1:2],
        down_square[None],
    )


def solution(mesh):
    return jax.shard_map(
        on_device,
        mesh=mesh,
        in_specs=(
            P("ep", None),
            P("ep", None),
            P("ep", None),
            P("ep", None),
            P("ep", None, "tp"),
            P("ep", None, "tp"),
            P("ep", "tp", None),
        ),
        out_specs=(
            P("ep", "tp"),
            P("ep", None),
            P("ep", None, "tp"),
            P("ep", None, "tp"),
            P("ep", "tp", None),
            P("ep", None),
            P("ep", None),
            P("ep", "tp"),
        ),
        check_vma=False,
    )
```

time: 193 us -> 150 us (0.78)
  Pallas kernels: 0 us -> 113 us
  blocking collectives: 93.2 us -> 0 us
  waiting for transfers between devices: 38.6 us -> 0 us
  between operations: 14 us -> 0.78 us
  local copies, waits for them, and re-layouts: 18.2 us -> 8.71 us
  starting transfers between devices: 5.75 us -> 0 us
  matrix products: 18.5 us -> 21.6 us
    pallas_call x0 -> x2, Pallas kernels: none -> 113 us  [the longest x1 69.7 us: dispatch(): pl.pallas_call(functools.partial(dispatch_kernel, experts, splits), out_s...]
    all_to_all x4 -> x0, blocking collectives: 84.9 us -> none  [the longest x1 32 us: on_device(): lax.all_to_all(outgoing, 'ep', split_axis=0, concat_axis=0, tiled=True)]
    all_gather x2 -> x0, waiting for transfers between devices: 18.4 us -> none  [the longest x1 18.4 us: on_device(): lax.all_gather(part_cot, 'tp', axis=1, tiled=True)]
    all_to_all x1 -> x0, waiting for transfers between devices: 12.3 us -> none  [on_device(): lax.all_to_all(reduced, 'ep', split_axis=0, concat_axis=0, tiled=True)]
    psum x1 -> x0, blocking collectives: 8.27 us -> none  [on_device(): lax.psum((route_part, gate_square, up_square), 'tp')]
    reduce_scatter x1 -> x0, waiting for transfers between devices: 7.87 us -> none  [on_device(): lax.psum_scatter(token_term.astype(jnp.bfloat16), 'tp', scatter_dimension...]
    gather x5 -> x0, local copies, waits for them, and re-layouts: 7.41 us -> none  [the longest x1 2.06 us: on_device(): outgoing = rows_pad[slot_owner]]
    all_to_all x1 -> x0, starting transfers between devices: 5.63 us -> none  [on_device(): lax.all_to_all(reduced, 'ep', split_axis=0, concat_axis=0, tiled=True)]
  transfers between devices with their start and end apart: 4 -> 0, of which waited for: 3 -> 0; matrix products, arithmetic and copies ran while one was open for 12% -> 0% of each run, Pallas kernels for 0% -> 0%
where the time goes in v1:
time: 150 us; the launch traced here: 147 us
  Pallas kernels  113 us (75%)
  matrix products  21.6 us (14%)
  local copies, waits for them, and re-layouts  8.71 us (6%)
  other arithmetic  2.87 us (2%)
    pallas_call x1, Pallas kernels, dispatch(): pl.pallas_call(functools.partial(dispatch_kernel, experts, splits), out_s...  69.7 us
    pallas_call x1, Pallas kernels, combine(): pl.pallas_call(functools.partial(combine_kernel, experts, splits), out_sh...  43.6 us
    dot_general x3, matrix products, outer(): lax.dot_general(left, right, (((0,), (0,)), ((), ())), preferred_element_...  7.04 us
    unnamed x18, local copies, waits for them, and re-layouts  4.2 us
    dot_general x2, matrix products, pack(): lax.dot_general(select, piece, (((0,), (0,)), ((), ())), preferred_elemen...  3.86 us

profile of v1, /device:TPU:0, one launch (start us, length us, event | category | flops | bytes accessed | tf_op | source)
XLA Modules:
  0.0 147.3 jit_solution(13978297963221993222)
XLA Ops:
  0.7 0.8 slice_bitcast_fusion.1
  1.5 0.7 bitcast_convert_fusion.1
  3.0 0.6 pad.7.scale_ref
  3.6 2.4 %convolution_convert_fusion.3 = bf16[512,1024]{1,0:T(8,128)(2,1)} fusion(pred[128,512]{1,0:T(32,128)(4,1)S(1)} %convolution_compare_fusion, bf16[128,2048]{1,0:T(8,128)(2,1)} %param.10, s32[]{:T(128)S(6)} %select_n.57), kind=kOutput, calls=%fused_computation.7 | convolution fusion | flops 134742016 | bytes 1376260 | tf_op jit(solution)/shard_map/dot_general | solution.py:285
  6.0 1.5 convolution_convert_fusion.4
  7.5 69.7 %shard_map.134 = (bf16[16,32,2048]{2,1,0:T(8,128)(2,1)}, bf16[16,32,2048]{2,1,0:T(8,128)(2,1)}, f32[16,1,128]{2,1,0:T(1,128)}) custom-call(bf16[16,32,1024]{2,1,0:T(8,128)(2,1)} %bitcast.61, bf16[16,32,1024]{2,1,0:T(8,128)(2,1)} %bitcast.60, f32[16,1,128]{2,1,0:T(1,128)} %pad.7.scale_ref), custom_call_target="tpu_custom_call" | custom-call | tf_op jit(solution)/shard_map/pallas_call | solution.py:121
  77.2 0.8 slice_reduce_fusion.1
  78.1 2.5 %fusion.4 = f32[512,256]{0,1:T(8,128)S(1)} fusion(bf16[512,2048]{1,0:T(8,128)(2,1)} %bitcast.71, bf16[1,2048,256]{2,1,0:T(8,128)(2,1)S(1)} %copy-done), kind=kOutput, calls=%fused_computation.17 | convolution fusion | flops 536870912 | bytes 3670016 | tf_op jit(solution)/shard_map/dot_general | solution.py:300
  80.7 0.8 fusion.7
  81.4 0.8 copy-done.6
  82.5 1.6 %multiply_reduce_fusion.3 = (f32[512]{0:T(512)S(1)}, bf16[512,256]{0,1:T(8,128)(2,1)S(1)}, bf16[512,256]{0,1:T(8,128)(2,1)}) fusion(f32[512,256]{0,1:T(8,128)S(1)} %fusion.7, f32[512,256]{0,1:T(8,128)S(1)} %fusion.4, f32[512]{0:T(512)S(1)} %mul.44, bf16[512,2048]{1,0:T(8,128)(2,1)S(1)} %bitcast.75, bf16[1,256,2048]{2,1,0:T(8,128)(2,1)S(1)} %copy-done.7), kind=kOutput, calls=%fused_computation.25 | convolution fusion | flops 539098624 | bytes 4722688 | tf_op jit(solution)/shard_map/dot_general | solution.py:302
  84.1 2.3 %multiply_reduce_fusion = (f32[256]{0:T(256)}, bf16[256,2048]{1,0:T(8,128)(2,1)}) fusion(bf16[512,2048]{1,0:T(8,128)(2,1)S(1)} %bitcast.76, f32[512]{0:T(512)S(1)} %mul.44, f32[512,256]{0,1:T(8,128)S(1)} %fusion.7, f32[512,256]{0,1:T(8,128)S(1)} %fusion.4), kind=kOutput, calls=%fused_computation.4 | convolution fusion | flops 539885312 | bytes 4197376 | tf_op jit(solution)/shard_map/dot_general | solution.py:315
  87.1 2.3 %multiply_reduce_fusion.2 = (f32[2048]{0:T(1024)S(1)}, bf16[2048,256]{0,1:T(8,128)(2,1)S(1)}) fusion(bf16[512,256]{0,1:T(8,128)(2,1)S(1)} %get-tuple-element.31, bf16[512,2048]{1,0:T(8,128)(2,1)} %bitcast.72), kind=kOutput, calls=%fused_computation.6 | convolution fusion | flops 538966016 | bytes 3416064 | tf_op jit(solution)/shard_map/dot_general | solution.py:315
  89.5 2.4 %multiply_reduce_fusion.1 = (f32[2048]{0:T(1024)S(1)}, bf16[2048,256]{0,1:T(8,128)(2,1)S(1)}) fusion(bf16[512,256]{0,1:T(8,128)(2,1)} %get-tuple-element.32, bf16[512,2048]{1,0:T(8,128)(2,1)} %bitcast.73), kind=kOutput, calls=%fused_computation.5 | convolution fusion | flops 538966016 | bytes 3416064 | tf_op jit(solution)/shard_map/dot_general | solution.py:315
  91.9 1.3 copy.16
  93.2 1.3 copy.15
  94.5 0.6 pad_maximum_fusion.square_ref
  95.1 0.8 fusion.2
  96.4 2.1 %add_convert_fusion = bf16[512,2048]{1,0:T(8,128)(2,1)} fusion(f32[512,2048]{1,0:T(8,128)S(1)} %fusion.2, bf16[512,256]{0,1:T(8,128)(2,1)S(1)} %copy-done.3, bf16[1,2048,256]{2,1,0:T(8,128)(2,1)S(1)} %copy-done.2), kind=kOutput, calls=%fused_computation | convolution fusion | flops 538968064 | bytes 7602176 | tf_op jit(solution)/shard_map/dot_general | solution.py:325
  98.5 43.6 %shard_map.135 = (bf16[16,32,1024]{2,1,0:T(8,128)(2,1)}, f32[16,1,128]{2,1,0:T(1,128)}, f32[1,2,2048]{2,1,0:T(2,128)}) custom-call(bf16[16,32,2048]{2,1,0:T(8,128)(2,1)} %bitcast.59, f32[16,1,128]{2,1,0:T(1,128)} %pad.8.route_ref, f32[2,2048]{1,0:T(2,128)} %pad_maximum_fusion.square_ref), custom_call_target="tpu_custom_call" | custom-call | tf_op jit(solution)/shard_map/pallas_call | solution.py:227
  142.1 0.7 bitcast_add_fusion
  142.9 2.2 %convolution_convert_fusion.5 = bf16[128,1024]{1,0:T(8,128)(2,1)} fusion(pred[128,512]{1,0:T(32,128)(4,1)S(1)} %convolution_compare_fusion, bf16[512,1024]{1,0:T(8,128)(2,1)} %bitcast.63), kind=kOutput, calls=%fused_computation.9 | convolution fusion | flops 134348800 | bytes 1376256 | tf_op jit(solution)/shard_map/dot_general | solution.py:338
  145.1 0.6 fusion.48
  145.7 0.7 slice_reduce_fusion
  (25 shorter events, 3.2 us)
Async XLA Ops:
  0.6 77.5 %copy-start = (bf16[1,2048,256]{2,1,0:T(8,128)(2,1)S(1)}, bf16[1,2048,256]{2,1,0:T(8,128)(2,1)}, u32[]{:S(2)}) copy-start(bf16[1,2048,256]{2,1,0:T(8,128)(2,1)} %param.11) | copy-start | bytes 3145732
  0.6 5.4 %copy-start.4 = (bf16[128,2048]{1,0:T(8,128)(2,1)S(1)}, bf16[128,2048]{1,0:T(8,128)(2,1)}, u32[]{:S(2)}) copy-start(bf16[128,2048]{1,0:T(8,128)(2,1)} %param.7) | copy-start | bytes 1572868
  77.2 3.4 %copy-start.1 = (bf16[1,2048,256]{2,1,0:T(8,128)(2,1)S(1)}, bf16[1,2048,256]{2,1,0:T(8,128)(2,1)}, u32[]{:S(2)}) copy-start(bf16[1,2048,256]{2,1,0:T(8,128)(2,1)} %param.12) | copy-start | bytes 3145732
  78.1 2.5 %copy-start.5 = (bf16[16,32,2048]{2,1,0:T(8,128)(2,1)S(1)}, bf16[16,32,2048]{2,1,0:T(8,128)(2,1)}, u32[]{:S(2)}) copy-start(bf16[16,32,2048]{2,1,0:T(8,128)(2,1)} %get-tuple-element.16) | copy-start | bytes 6291460
  80.6 1.6 %copy-start.6 = (bf16[16,32,2048]{2,1,0:T(8,128)(2,1)S(1)}, bf16[16,32,2048]{2,1,0:T(8,128)(2,1)}, u32[]{:S(2)}) copy-start(bf16[16,32,2048]{2,1,0:T(8,128)(2,1)} %get-tuple-element.15) | copy-start | bytes 6291460
  80.6 1.8 %copy-start.7 = (bf16[1,256,2048]{2,1,0:T(8,128)(2,1)S(1)}, bf16[1,256,2048]{2,1,0:T(8,128)(2,1)}, u32[]{:S(2)}) copy-start(bf16[1,256,2048]{2,1,0:T(8,128)(2,1)} %param.13) | copy-start | bytes 3145732
  95.1 1.2 copy-start.2
  95.1 1.3 copy-start.3

commit v2 on v1

--- a/solution.py
+++ b/solution.py
@@ -9,6 +9,8 @@
 
 MESH = pl.DeviceIdType.MESH
 LANES = 128
+SHARE = 4
+GROUPS = 4
 
 
 def greet(experts, splits, me, col):
@@ -39,99 +41,175 @@
 
 
 def dispatch_kernel(
-    experts, splits, rows_ref, cot_ref, scale_ref, rows_out, cot_out, scale_out,
-    send, recv, relay_send, relay_recv, local,
+    experts, splits, rows_ref, cot_ref, choice_ref, scale_ref, rows_out, cot_out, scale_out,
+    landed, landed_choice, stage, far_send, far_recv, send, recv, relay_send, relay_recv,
+    scale_send, scale_recv, local,
 ):
     me = lax.axis_index("ep")
     col = lax.axis_index("tp")
-    width = rows_ref.shape[2]
+    members = experts // GROUPS
+    group = me // members
+    seat = lax.rem(me, members)
+    model_width = rows_out.shape[2]
+    capacity = rows_out.shape[1]
+    packed = rows_ref.shape[2]
+    width = (model_width - packed) // (splits - 1) if splits > 1 else model_width
+    shared = model_width - splits * width
     mine = pl.ds(pl.multiple_of(col * width, LANES), width)
     greet(experts, splits, me, col)
-    pairs = ((rows_ref, rows_out), (cot_ref, cot_out))
-
-    def out_copies(off):
+    inputs = (rows_ref, cot_ref, choice_ref)
+    outputs = (rows_out, cot_out)
+    views = [(i, pl.ds(0, width), mine) for i in range(2)]
+    if shared:
+        views += [(i, pl.ds(width, shared), pl.ds(splits * width, shared)) for i in range(2)]
+
+    def far_copy(step, i):
+        there = lax.rem(group + step, GROUPS)
+        target = landed_choice.at[step] if i == 2 else landed.at[i, step]
+        return remote(
+            inputs[i].at[there], target, far_send.at[i, step], far_recv.at[i, step],
+            there * members + seat, col,
+        )
+
+    def origin(step, hop):
+        return lax.rem(group + GROUPS - step, GROUPS) * members + lax.rem(seat + members - hop, members)
+
+    def near_copy(step, hop, n):
+        i, here, there = views[n]
+        target = lax.rem(seat + hop, members)
+        return remote(
+            stage.at[i, step, target, :, here], outputs[i].at[origin(step, 0), :, there],
+            send.at[n, step, hop], recv.at[n, step, hop], group * members + target, col,
+        )
+
+    def own_copy(step, n):
+        i, here, there = views[n]
+        return pltpu.make_async_copy(
+            stage.at[i, step, seat, :, here], outputs[i].at[origin(step, 0), :, there], local.at[n, step]
+        )
+
+    def relay(step, hop, shift, i, part):
+        block = outputs[i].at[origin(step, hop), :, part]
+        peer = lax.rem(col + shift, splits)
+        return remote(
+            block, block, relay_send.at[i, shift - 1, step, hop], relay_recv.at[i, shift - 1, step, hop], me, peer
+        )
+
+    def scale_copy(off):
         there = lax.rem(me + off, experts)
-        copies = [
-            remote(src.at[there], dst.at[me, :, mine], send.at[i, off], recv.at[i, off], there, col)
-            for i, (src, dst) in enumerate(pairs)
-        ]
-        copies.append(
-            remote(scale_ref.at[there], scale_out.at[me], send.at[2, off], recv.at[2, off], there, col)
-        )
-        return copies
-
-    def relays(off, shift, i):
-        source = lax.rem(me + experts - off, experts)
-        block = pairs[i][1].at[source, :, mine]
-        peer = lax.rem(col + shift, splits)
-        return remote(block, block, relay_send.at[i, shift - 1, off], relay_recv.at[i, shift - 1, off], me, peer)
-
-    own = [
-        pltpu.make_async_copy(src.at[me], dst.at[me, :, mine], local.at[i])
-        for i, (src, dst) in enumerate(pairs)
-    ]
-    own.append(pltpu.make_async_copy(scale_ref.at[me], scale_out.at[me], local.at[2]))
-    for copy in own:
-        copy.start()
+        return remote(
+            scale_ref.at[there], scale_out.at[me], scale_send.at[off], scale_recv.at[off], there, col
+        )
+
+    scale_own = pltpu.make_async_copy(scale_ref.at[me], scale_out.at[me], local.at[4, 0])
+    for step in range(1, GROUPS):
+        for i in (2, 0, 1):
+            far_copy(step, i).start()
+    scale_own.start()
+
+    for step in range(GROUPS):
+        if step:
+            far_copy(step, 2).wait_recv()
+            choice = landed_choice[step]
+        else:
+            choice = choice_ref[group]
+        for i in range(2):
+            if step:
+                far_copy(step, i).wait_recv()
+                block = landed[i, step]
+            else:
+                block = inputs[i][group]
+            spread = lax.dot_general(
+                choice, block, (((0,), (0,)), ((), ())), preferred_element_type=jnp.float32
+            )
+            stage[i, step] = spread.astype(jnp.bfloat16).reshape(members, capacity, packed)
+            for n in range(i, len(views), 2):
+                own_copy(step, n).start()
+
+            @pl.loop(1, members)
+            def _(hop):
+                near_copy(step, hop, i).start()
+
+            if shared:
+
+                @pl.loop(1, members)
+                def _(hop):
+                    near_copy(step, hop, i + 2).start()
+
+        if step == 0:
+
+            @pl.loop(1, experts)
+            def _(off):
+                scale_copy(off).start()
+
+        for n in range(len(views)):
+            own_copy(step, n).wait()
+        for i in range(2):
+            for shift in range(1, splits):
+                relay(step, 0, shift, i, mine).start()
+
+        @pl.loop(1, members)
+        def _(hop):
+            for i in range(2):
+                near_copy(step, hop, i).wait_recv()
+                for shift in range(1, splits):
+                    relay(step, hop, shift, i, mine).start()
+
+    scale_own.wait()
 
     @pl.loop(1, experts)
     def _(off):
-        for copy in out_copies(off):
-            copy.start()
-
-    for copy in own:
-        copy.wait()
-    for shift in range(1, splits):
-        for i in range(2):
-            relays(0, shift, i).start()
-
-    @pl.loop(1, experts)
-    def _(off):
-        copies = out_copies(off)
-        for i in range(2):
-            copies[i].wait_recv()
+        scale_copy(off).wait()
+
+    for step in range(GROUPS):
+        if step:
+            for i in range(3):
+                far_copy(step, i).wait_send()
+
+        @pl.loop(1, members)
+        def _(hop):
+            for n in range(len(views)):
+                near_copy(step, hop, n).wait_send()
+                if n >= 2:
+                    near_copy(step, hop, n).wait_recv()
+
+        @pl.loop(0, members)
+        def _(hop):
             for shift in range(1, splits):
-                relays(off, shift, i).start()
-
-    @pl.loop(1, experts)
-    def _(off):
-        copies = out_copies(off)
-        for copy in copies:
-            copy.wait_send()
-        copies[2].wait_recv()
-
-    @pl.loop(0, experts)
-    def _(off):
-        for shift in range(1, splits):
-            for i in range(2):
-                relays(off, shift, i).wait_send()
-                source = lax.rem(me + experts - off, experts)
-                peer = lax.rem(col + splits - shift, splits)
-                part = pl.ds(pl.multiple_of(peer * width, LANES), width)
-                block = pairs[i][1].at[source, :, part]
-                remote(
-                    block, block, relay_send.at[i, shift - 1, off], relay_recv.at[i, shift - 1, off], me, peer
-                ).wait_recv()
-
-
-def dispatch(rows, cot, scale, experts, splits):
-    capacity, width = rows.shape[1:]
-    whole = jax.ShapeDtypeStruct((experts, capacity, width * splits), jnp.bfloat16)
+                for i in range(2):
+                    relay(step, hop, shift, i, mine).wait_send()
+                    peer = lax.rem(col + splits - shift, splits)
+                    part = pl.ds(pl.multiple_of(peer * width, LANES), width)
+                    relay(step, hop, shift, i, part).wait_recv()
+
+
+def dispatch(rows, cot, choice, scale, model_width, experts, splits):
+    members = experts // GROUPS
+    capacity = choice.shape[2] // members
+    whole = jax.ShapeDtypeStruct((experts, capacity, model_width), jnp.bfloat16)
     vmem = pl.BlockSpec(memory_space=pltpu.VMEM)
+    dma = pltpu.SemaphoreType.DMA
     return pl.pallas_call(
         functools.partial(dispatch_kernel, experts, splits),
         out_shape=(whole, whole, jax.ShapeDtypeStruct(scale.shape, scale.dtype)),
-        in_specs=[vmem] * 3,
+        in_specs=[vmem] * 4,
         out_specs=(vmem,) * 3,
         scratch_shapes=[
-            pltpu.SemaphoreType.DMA((3, experts)),
-            pltpu.SemaphoreType.DMA((3, experts)),
-            pltpu.SemaphoreType.DMA((2, splits - 1, experts)),
-            pltpu.SemaphoreType.DMA((2, splits - 1, experts)),
-            pltpu.SemaphoreType.DMA((3,)),
+            pltpu.VMEM((2,) + rows.shape, jnp.bfloat16),
+            pltpu.VMEM(choice.shape, jnp.bfloat16),
+            pltpu.VMEM((2, GROUPS, members, capacity, rows.shape[2]), jnp.bfloat16),
+            dma((3, GROUPS)),
+            dma((3, GROUPS)),
+            dma((4, GROUPS, members)),
+            dma((4, GROUPS, members)),
+            dma((2, splits - 1, GROUPS, members)),
+            dma((2, splits - 1, GROUPS, members)),
+            dma((experts,)),
+            dma((experts,)),
+            dma((5, GROUPS)),
         ],
         compiler_params=pltpu.CompilerParams(collective_id=0, has_side_effects=True),
-    )(rows, cot, scale)
+    )(rows, cot, choice, scale)
 
 
 def combine_kernel(
@@ -277,18 +355,43 @@
     slot_weight = jnp.sum(
         jnp.where(chosen, jnp.dot(weight, spread, preferred_element_type=f32), 0.0), axis=0
     )
+    members = experts // GROUPS
+    group_cap = members * capacity // topk
+    group_slots = jnp.arange(GROUPS * group_cap, dtype=jnp.int32)[None, :]
+    group_iota = jnp.arange(GROUPS, dtype=jnp.int32)[None, :]
+    in_group = expert_ids[:, :1] // members == group_iota
+    group_before = jnp.dot(earlier, in_group.astype(bf16), preferred_element_type=f32)
+    own_rank = jnp.sum(jnp.where(in_group, group_before, 0.0), axis=1, keepdims=True).astype(jnp.int32)
+    own_slot = expert_ids[:, :1] // members * group_cap + own_rank
+    group_select = (own_slot == group_slots).astype(bf16)
+    grouped = lax.dot_general(
+        group_select, select, (((0,), (0,)), ((), ())), preferred_element_type=f32
+    ).astype(bf16)
+    span = members * capacity
+    choice = jnp.stack(
+        [
+            grouped[g * group_cap : (g + 1) * group_cap, g * span : (g + 1) * span]
+            for g in range(GROUPS)
+        ]
+    )
     width = model_width // splits
-    start = lax.axis_index("tp") * width
+    shared = model_width // SHARE // (splits * LANES) * (splits * LANES) if SHARE else 0
+    cut = (model_width - shared) // splits
+    start = lax.axis_index("tp") * cut
 
     def pack(array):
-        piece = lax.dynamic_slice_in_dim(array, start, width, 1)
-        packed = lax.dot_general(select, piece, (((0,), (0,)), ((), ())), preferred_element_type=f32)
-        return packed.astype(bf16).reshape(experts, capacity, width)
+        piece = jnp.concatenate(
+            [lax.dynamic_slice_in_dim(array, start, cut, 1), array[:, splits * cut :]], axis=1
+        )
+        packed = lax.dot_general(
+            group_select, piece, (((0,), (0,)), ((), ())), preferred_element_type=f32
+        )
+        return packed.astype(bf16).reshape(GROUPS, group_cap, cut + shared)
 
     lane_pad = -capacity % LANES
     scale_out = jnp.pad(slot_weight.reshape(experts, 1, capacity), ((0, 0), (0, 0), (0, lane_pad)))
     slot_rows, slot_cot, got_scale = dispatch(
-        pack(tokens), pack(cotangent), scale_out, experts, splits
+        pack(tokens), pack(cotangent), choice, scale_out, model_width, experts, splits
     )
     slot_rows = slot_rows.reshape(slot_count, model_width)
     slot_cot = slot_cot.reshape(slot_count, model_width)

time: 150 us -> 131 us (0.87)
  Pallas kernels: 113 us -> 94.1 us
  other arithmetic: 2.87 us -> 4.38 us
    pallas_call x1, Pallas kernels: 69.7 us -> 55 us  [dispatch(): pl.pallas_call(functools.partial(dispatch_kernel, experts, splits), out_s...]
    pallas_call x1, Pallas kernels: 43.6 us -> 39.2 us  [combine(): pl.pallas_call(functools.partial(combine_kernel, experts, splits), out_sh...]
    dot_general x2 -> x4, matrix products: 3.86 us -> 3.05 us  [the longest x2 2.57 us: pack(): lax.dot_general(group_select, piece, (((0,), (0,)), ((), ())), preferred_...]
    unnamed x18 -> x20, local copies, waits for them, and re-layouts: 4.2 us -> 4.2 us
where the time goes in v2:
time: 131 us; the launch traced here: 128 us
  Pallas kernels  94.1 us (72%)
  matrix products  20.8 us (16%)
  local copies, waits for them, and re-layouts  7.95 us (6%)
  other arithmetic  4.38 us (3%)
    pallas_call x1, Pallas kernels, dispatch(): pl.pallas_call(functools.partial(dispatch_kernel, experts, splits), out_s...  55 us
    pallas_call x1, Pallas kernels, combine(): pl.pallas_call(functools.partial(combine_kernel, experts, splits), out_sh...  39.2 us
    dot_general x3, matrix products, outer(): lax.dot_general(left, right, (((0,), (0,)), ((), ())), preferred_element_...  7.02 us
    unnamed x20, local copies, waits for them, and re-layouts  4.2 us

profile of v2, /device:TPU:0, one launch (start us, length us, event | category | flops | bytes accessed | tf_op | source)
XLA Modules:
  0.0 128.1 jit_solution(15014174868182268376)
XLA Ops:
  0.7 0.8 bitcast_convert_fusion.1
  1.5 0.8 and_select_fusion
  3.2 0.6 pad.7.scale_ref
  4.2 0.6 pad_maximum_fusion.choice_ref
  4.9 1.3 %convolution_convert_fusion.3 = bf16[256,1280]{1,0:T(8,128)(2,1)} fusion(bf16[128,512]{1,0:T(8,128)(2,1)S(1)} %slice-done.1, bf16[128,768]{1,0:T(8,128)(2,1)S(1)} %get-tuple-element.52, s32[128]{0:T(128)S(1)} %fusion.51), kind=kOutput, calls=%fused_computation.4 | convolution fusion | flops 84901888 | bytes 983552 | tf_op jit(solution)/shard_map/dot_general | solution.py:386
  6.2 1.3 %convolution_convert_fusion.4 = bf16[256,1280]{1,0:T(8,128)(2,1)} fusion(bf16[128,512]{1,0:T(8,128)(2,1)S(1)} %slice-done, bf16[128,768]{1,0:T(8,128)(2,1)S(1)} %get-tuple-element.53, s32[128]{0:T(128)S(1)} %fusion.51), kind=kOutput, calls=%fused_computation.5 | convolution fusion | flops 84901888 | bytes 983552 | tf_op jit(solution)/shard_map/dot_general | solution.py:386
  7.5 55.0 %shard_map.134 = (bf16[16,32,2048]{2,1,0:T(8,128)(2,1)}, bf16[16,32,2048]{2,1,0:T(8,128)(2,1)}, f32[16,1,128]{2,1,0:T(1,128)}) custom-call(bf16[4,64,1280]{2,1,0:T(8,128)(2,1)} %bitcast.75, bf16[4,64,1280]{2,1,0:T(8,128)(2,1)} %bitcast.74, bf16[4,64,128]{2,1,0:T(8,128)(2,1)} %pad_maximum_fusion.choice_ref, f32[16,1,128]{2,1,0:T(1,128)} %pad.7.scale_ref), custom_call_target="tpu_custom_call" | custom-call | tf_op jit(solution)/shard_map/pallas_call | solution.py:192
  62.5 0.8 slice_reduce_fusion.1
  63.4 2.5 %fusion.5 = f32[512,256]{0,1:T(8,128)S(1)} fusion(bf16[512,2048]{1,0:T(8,128)(2,1)} %bitcast.86, bf16[1,2048,256]{2,1,0:T(8,128)(2,1)S(1)} %copy-done), kind=kOutput, calls=%fused_computation.20 | convolution fusion | flops 536870912 | bytes 3670016 | tf_op jit(solution)/shard_map/dot_general | solution.py:403
  65.9 0.8 fusion.8
  66.7 0.8 copy-done.7
  67.7 1.7 %multiply_reduce_fusion.3 = (f32[512]{0:T(512)S(1)}, bf16[512,256]{0,1:T(8,128)(2,1)S(1)}, bf16[512,256]{0,1:T(8,128)(2,1)}) fusion(f32[512,256]{0,1:T(8,128)S(1)} %fusion.8, f32[512,256]{0,1:T(8,128)S(1)} %fusion.5, f32[512]{0:T(512)S(1)} %mul.52, bf16[512,2048]{1,0:T(8,128)(2,1)S(1)} %bitcast.90, bf16[1,256,2048]{2,1,0:T(8,128)(2,1)S(1)} %copy-done.8), kind=kOutput, calls=%fused_computation.28 | convolution fusion | flops 539098624 | bytes 4722688 | tf_op jit(solution)/shard_map/dot_general | solution.py:405
  69.4 2.3 %multiply_reduce_fusion = (f32[256]{0:T(256)}, bf16[256,2048]{1,0:T(8,128)(2,1)}) fusion(bf16[512,2048]{1,0:T(8,128)(2,1)S(1)} %bitcast.91, f32[512]{0:T(512)S(1)} %mul.52, f32[512,256]{0,1:T(8,128)S(1)} %fusion.8, f32[512,256]{0,1:T(8,128)S(1)} %fusion.5), kind=kOutput, calls=%fused_computation.6 | convolution fusion | flops 539885312 | bytes 4197376 | tf_op jit(solution)/shard_map/dot_general | solution.py:418
  72.4 2.3 %multiply_reduce_fusion.2 = (f32[2048]{0:T(1024)S(1)}, bf16[2048,256]{0,1:T(8,128)(2,1)S(1)}) fusion(bf16[512,256]{0,1:T(8,128)(2,1)S(1)} %get-tuple-element.31, bf16[512,2048]{1,0:T(8,128)(2,1)} %bitcast.87), kind=kOutput, calls=%fused_computation.8 | convolution fusion | flops 538966016 | bytes 3416064 | tf_op jit(solution)/shard_map/dot_general | solution.py:418
  74.7 2.4 %multiply_reduce_fusion.1 = (f32[2048]{0:T(1024)S(1)}, bf16[2048,256]{0,1:T(8,128)(2,1)S(1)}) fusion(bf16[512,256]{0,1:T(8,128)(2,1)} %get-tuple-element.32, bf16[512,2048]{1,0:T(8,128)(2,1)} %bitcast.88), kind=kOutput, calls=%fused_computation.7 | convolution fusion | flops 538966016 | bytes 3416064 | tf_op jit(solution)/shard_map/dot_general | solution.py:418
  77.1 1.3 %copy.16 = bf16[1,2048,256]{2,1,0:T(8,128)(2,1)} copy(bf16[1,2048,256]{1,2,0:T(8,128)(2,1)S(1)} %bitcast.78) | data formatting | bytes 2097152
  78.5 1.3 %copy.15 = bf16[1,2048,256]{2,1,0:T(8,128)(2,1)} copy(bf16[1,2048,256]{1,2,0:T(8,128)(2,1)S(1)} %bitcast.76) | data formatting | bytes 2097152
  80.4 0.8 fusion.3
  81.6 2.2 %add_convert_fusion = bf16[512,2048]{1,0:T(8,128)(2,1)} fusion(f32[512,2048]{1,0:T(8,128)S(1)} %fusion.3, bf16[512,256]{0,1:T(8,128)(2,1)S(1)} %copy-done.5, bf16[1,2048,256]{2,1,0:T(8,128)(2,1)S(1)} %copy-done.2), kind=kOutput, calls=%fused_computation | convolution fusion | flops 538968064 | bytes 7602176 | tf_op jit(solution)/shard_map/dot_general | solution.py:428
  83.8 39.2 %shard_map.135 = (bf16[16,32,1024]{2,1,0:T(8,128)(2,1)}, f32[16,1,128]{2,1,0:T(1,128)}, f32[1,2,2048]{2,1,0:T(2,128)}) custom-call(bf16[16,32,2048]{2,1,0:T(8,128)(2,1)} %bitcast.73, f32[16,1,128]{2,1,0:T(1,128)} %pad.8.route_ref, f32[2,2048]{1,0:T(2,128)} %pad_maximum_fusion.1.square_ref), custom_call_target="tpu_custom_call" | custom-call | tf_op jit(solution)/shard_map/pallas_call | solution.py:305
  123.0 0.7 bitcast_add_fusion
  123.7 2.2 %convolution_convert_fusion.6 = bf16[128,1024]{1,0:T(8,128)(2,1)} fusion(pred[128,512]{1,0:T(32,128)(4,1)S(1)} %convolution_compare_fusion, bf16[512,1024]{1,0:T(8,128)(2,1)} %bitcast.77), kind=kOutput, calls=%fused_computation.10 | convolution fusion | flops 134348800 | bytes 1376256 | tf_op jit(solution)/shard_map/dot_general | solution.py:441
  125.9 0.6 fusion.58
  126.6 0.7 slice_reduce_fusion
  (37 shorter events, 4.3 us)
Async XLA Ops:
  0.6 62.7 %copy-start = (bf16[1,2048,256]{2,1,0:T(8,128)(2,1)S(1)}, bf16[1,2048,256]{2,1,0:T(8,128)(2,1)}, u32[]{:S(2)}) copy-start(bf16[1,2048,256]{2,1,0:T(8,128)(2,1)} %param.11) | copy-start | bytes 3145732
  0.6 4.2 %copy-start.4 = (bf16[128,2048]{1,0:T(8,128)(2,1)S(1)}, bf16[128,2048]{1,0:T(8,128)(2,1)}, u32[]{:S(2)}) copy-start(bf16[128,2048]{1,0:T(8,128)(2,1)} %param.10) | copy-start | bytes 1572868
  0.7 4.2 %slice-start.1 = ((bf16[128,2048]{1,0:T(8,128)(2,1)}), bf16[128,512]{1,0:T(8,128)(2,1)S(1)}, s32[]{:S(2)}) async-start(bf16[128,2048]{1,0:T(8,128)(2,1)} %param.10), calls=%async_computation.1 | async-start | bytes 262144 | tf_op jit(solution)/shard_map/slice | solution.py:384
  0.7 4.2 %copy-start.3 = (bf16[128,2048]{1,0:T(8,128)(2,1)S(1)}, bf16[128,2048]{1,0:T(8,128)(2,1)}, u32[]{:S(2)}) copy-start(bf16[128,2048]{1,0:T(8,128)(2,1)} %param.7) | copy-start | bytes 1572868
  0.7 5.5 %slice-start = ((bf16[128,2048]{1,0:T(8,128)(2,1)}), bf16[128,512]{1,0:T(8,128)(2,1)S(1)}, s32[]{:S(2)}) async-start(bf16[128,2048]{1,0:T(8,128)(2,1)} %param.7), calls=%async_computation | async-start | bytes 262144 | tf_op jit(solution)/shard_map/slice | solution.py:384
  62.5 3.4 %copy-start.1 = (bf16[1,2048,256]{2,1,0:T(8,128)(2,1)S(1)}, bf16[1,2048,256]{2,1,0:T(8,128)(2,1)}, u32[]{:S(2)}) copy-start(bf16[1,2048,256]{2,1,0:T(8,128)(2,1)} %param.12) | copy-start | bytes 3145732
  63.4 2.5 %copy-start.6 = (bf16[16,32,2048]{2,1,0:T(8,128)(2,1)S(1)}, bf16[16,32,2048]{2,1,0:T(8,128)(2,1)}, u32[]{:S(2)}) copy-start(bf16[16,32,2048]{2,1,0:T(8,128)(2,1)} %get-tuple-element.16) | copy-start | bytes 6291460
  65.9 1.6 %copy-start.7 = (bf16[16,32,2048]{2,1,0:T(8,128)(2,1)S(1)}, bf16[16,32,2048]{2,1,0:T(8,128)(2,1)}, u32[]{:S(2)}) copy-start(bf16[16,32,2048]{2,1,0:T(8,128)(2,1)} %get-tuple-element.15) | copy-start | bytes 6291460
  65.9 1.8 %copy-start.8 = (bf16[1,256,2048]{2,1,0:T(8,128)(2,1)S(1)}, bf16[1,256,2048]{2,1,0:T(8,128)(2,1)}, u32[]{:S(2)}) copy-start(bf16[1,256,2048]{2,1,0:T(8,128)(2,1)} %param.13) | copy-start | bytes 3145732
  80.4 1.2 copy-start.2
  80.4 1.3 copy-start.5

commit v3 on v2

--- a/solution.py
+++ b/solution.py
@@ -41,8 +41,8 @@
 
 
 def dispatch_kernel(
-    experts, splits, rows_ref, cot_ref, choice_ref, scale_ref, rows_out, cot_out, scale_out,
-    landed, landed_choice, stage, far_send, far_recv, send, recv, relay_send, relay_recv,
+    experts, splits, rows_ref, cot_ref, choice_ref, scale_ref, rows_out, cot_out, scale_out, landed_choice,
+    landed, stage, far_send, far_recv, send, recv, relay_send, relay_recv,
     scale_send, scale_recv, local,
 ):
     me = lax.axis_index("ep")
@@ -106,6 +106,8 @@
         for i in (2, 0, 1):
             far_copy(step, i).start()
     scale_own.start()
+    choice_own = pltpu.make_async_copy(choice_ref.at[group], landed_choice.at[0], local.at[4, 1])
+    choice_own.start()
 
     for step in range(GROUPS):
         if step:
@@ -156,6 +158,7 @@
                     relay(step, hop, shift, i, mine).start()
 
     scale_own.wait()
+    choice_own.wait()
 
     @pl.loop(1, experts)
     def _(off):
@@ -191,12 +194,12 @@
     dma = pltpu.SemaphoreType.DMA
     return pl.pallas_call(
         functools.partial(dispatch_kernel, experts, splits),
-        out_shape=(whole, whole, jax.ShapeDtypeStruct(scale.shape, scale.dtype)),
+        out_shape=(whole, whole, jax.ShapeDtypeStruct(scale.shape, scale.dtype),
+                   jax.ShapeDtypeStruct(choice.shape, choice.dtype)),
         in_specs=[vmem] * 4,
-        out_specs=(vmem,) * 3,
+        out_specs=(vmem,) * 4,
         scratch_shapes=[
             pltpu.VMEM((2,) + rows.shape, jnp.bfloat16),
-            pltpu.VMEM(choice.shape, jnp.bfloat16),
             pltpu.VMEM((2, GROUPS, members, capacity, rows.shape[2]), jnp.bfloat16),
             dma((3, GROUPS)),
             dma((3, GROUPS)),
@@ -213,23 +216,32 @@
 
 
 def combine_kernel(
-    experts, splits, part_ref, route_ref, square_ref, back, back_route, square_out,
-    peer_part, total, peer_route, route_total,
-    swap_send, swap_recv, small_send, small_recv, send, recv,
+    experts, splits, part_ref, route_ref, square_ref, choice_ref, back, back_route, square_out,
+    peer_part, total, gathered, finished, peer_route, route_total,
+    swap_send, swap_recv, small_send, small_recv, near_send, near_recv, far_send, far_recv,
+    route_send, route_recv,
 ):
     me = lax.axis_index("ep")
     col = lax.axis_index("tp")
+    members = experts // GROUPS
+    group = me // members
+    seat = lax.rem(me, members)
+    capacity = part_ref.shape[1]
     width = back.shape[2]
     mine = pl.ds(pl.multiple_of(col * width, LANES), width)
     greet(experts, splits, me, col)
-
-    def swap(off, shift):
-        source = lax.rem(me + off, experts)
+    order = tuple(range(1, GROUPS)) + (0,)
+
+    def home(step, hop):
+        return lax.rem(group + GROUPS - step, GROUPS) * members + lax.rem(seat + hop, members)
+
+    def swap(step, hop, shift):
+        source = home(step, hop)
         peer = lax.rem(col + shift, splits)
         theirs = pl.ds(pl.multiple_of(peer * width, LANES), width)
         return remote(
             part_ref.at[source, :, theirs], peer_part.at[shift - 1, source],
-            swap_send.at[shift - 1, off], swap_recv.at[shift - 1, off], me, peer,
+            swap_send.at[shift - 1, step, hop], swap_recv.at[shift - 1, step, hop], me, peer,
         )
 
     small = []
@@ -244,28 +256,41 @@
     for shift in range(1, splits):
         small[shift - 1][0].start()
 
-    @pl.loop(1, experts + 1)
-    def _(step):
-        for shift in range(1, splits):
-            swap(lax.rem(step, experts), shift).start()
+    for step in order:
+
+        @pl.loop(1, members + 1)
+        def _(turn):
+            for shift in range(1, splits):
+                swap(step, lax.rem(turn, members), shift).start()
 
     for shift in range(1, splits):
         small[shift - 1][1].start()
 
-    def block_total(off):
-        source = lax.rem(me + off, experts)
+    def block_total(step, hop):
+        source = home(step, hop)
         for shift in range(1, splits):
-            swap(off, shift).wait_recv()
+            swap(step, hop, shift).wait_recv()
         value = part_ref[source, :, mine].astype(jnp.float32)
         for shift in range(1, splits):
             value = value + peer_part[shift - 1, source].astype(jnp.float32)
         return value.astype(back.dtype)
 
-    def out_copies(off):
+    def near_copy(step, hop):
+        target = lax.rem(seat + hop, members)
+        return remote(
+            total.at[step, hop], gathered.at[step, seat],
+            near_send.at[step, hop], near_recv.at[step, hop], group * members + target, col,
+        )
+
+    def far_copy(step):
+        return remote(
+            finished.at[step], back.at[group], far_send.at[step], far_recv.at[step], home(step, 0), col
+        )
+
+    def route_copy(off):
         there = lax.rem(me + off, experts)
-        return (
-            remote(total.at[there], back.at[me], send.at[0, off], recv.at[0, off], there, col),
-            remote(route_total.at[there], back_route.at[me], send.at[1, off], recv.at[1, off], there, col),
+        return remote(
+            route_total.at[there], back_route.at[me], route_send.at[off], route_recv.at[off], there, col
         )
 
     value = route_ref[...]
@@ -277,54 +302,93 @@
 
     @pl.loop(1, experts)
     def _(off):
-        total[lax.rem(me + off, experts)] = block_total(off)
-        for copy in out_copies(off):
-            copy.start()
-
-    back[me] = block_total(0)
+        route_copy(off).start()
+
+    def spread(step):
+        @pl.loop(1, members)
+        def _(hop):
+            total[step, hop] = block_total(step, hop)
+            near_copy(step, hop).start()
+
+        gathered[step, seat] = block_total(step, 0)
+
+    def collect(step):
+        @pl.loop(1, members)
+        def _(hop):
+            near_copy(step, hop).wait_recv()
+
+        pairs = gathered[step].reshape(members * capacity, width)
+        summed = jnp.dot(choice_ref[step], pairs, preferred_element_type=jnp.float32).astype(back.dtype)
+        if step:
+            finished[step] = summed
+            far_copy(step).start()
+        else:
+            back[group] = summed
+
+    for turn, step in enumerate(order):
+        spread(step)
+        if turn:
+            collect(order[turn - 1])
+    collect(order[-1])
 
     @pl.loop(1, experts)
     def _(off):
-        for copy in out_copies(off):
-            copy.wait()
-
-    @pl.loop(0, experts)
-    def _(off):
-        for shift in range(1, splits):
-            swap(off, shift).wait_send()
+        route_copy(off).wait()
+
+    for step in range(GROUPS):
+        if step:
+            far_copy(step).wait()
+
+        @pl.loop(1, members)
+        def _(hop):
+            near_copy(step, hop).wait_send()
+
+        @pl.loop(0, members)
+        def _(hop):
+            for shift in range(1, splits):
+                swap(step, hop, shift).wait_send()
 
     for shift in range(1, splits):
         small[shift - 1][0].wait_send()
         small[shift - 1][1].wait()
 
 
-def combine(part, route, squares, experts, splits):
+def combine(part, route, squares, choice, experts, splits):
     capacity, model_width = part.shape[1:]
     width = model_width // splits
+    members = experts // GROUPS
+    group_cap = choice.shape[1]
     vmem = pl.BlockSpec(memory_space=pltpu.VMEM)
+    dma = pltpu.SemaphoreType.DMA
     return pl.pallas_call(
         functools.partial(combine_kernel, experts, splits),
         out_shape=(
-            jax.ShapeDtypeStruct((experts, capacity, width), jnp.bfloat16),
+            jax.ShapeDtypeStruct((GROUPS, group_cap, width), jnp.bfloat16),
             jax.ShapeDtypeStruct(route.shape, jnp.float32),
             jax.ShapeDtypeStruct((splits - 1,) + squares.shape, jnp.float32),
         ),
-        in_specs=[vmem] * 3,
+        in_specs=[vmem] * 4,
         out_specs=(vmem,) * 3,
         scratch_shapes=[
             pltpu.VMEM((splits - 1, experts, capacity, width), jnp.bfloat16),
-            pltpu.VMEM((experts, capacity, width), jnp.bfloat16),
+            pltpu.VMEM((GROUPS, members, capacity, width), jnp.bfloat16),
+            pltpu.VMEM((GROUPS, members, capacity, width), jnp.bfloat16),
+            pltpu.VMEM((GROUPS, group_cap, width), jnp.bfloat16),
             pltpu.VMEM((splits - 1,) + route.shape, jnp.float32),
             pltpu.VMEM(route.shape, jnp.float32),
-            pltpu.SemaphoreType.DMA((splits - 1, experts)),
-            pltpu.SemaphoreType.DMA((splits - 1, experts)),
-            pltpu.SemaphoreType.DMA((2, splits - 1)),
-            pltpu.SemaphoreType.DMA((2, splits - 1)),
-            pltpu.SemaphoreType.DMA((2, experts)),
-            pltpu.SemaphoreType.DMA((2, experts)),
+            dma((splits - 1, GROUPS, members)),
+            dma((splits - 1, GROUPS, members)),
+            dma((2, splits - 1)),
+            dma((2, splits - 1)),
+            dma((GROUPS, members)),
+            dma((GROUPS, members)),
+            dma((GROUPS,)),
+            dma((GROUPS,)),
+            dma((experts,)),
+            dma((experts,)),
         ],
         compiler_params=pltpu.CompilerParams(collective_id=1, has_side_effects=True),
-    )(part, route, squares)
+    )(part, route, squares, choice)
 
 
 def on_device(tokens, expert_ids, route_weights, cotangent, w_gate, w_up, w_down):
@@ -390,7 +454,7 @@
 
     lane_pad = -capacity % LANES
     scale_out = jnp.pad(slot_weight.reshape(experts, 1, capacity), ((0, 0), (0, 0), (0, lane_pad)))
-    slot_rows, slot_cot, got_scale = dispatch(
+    slot_rows, slot_cot, got_scale, got_choice = dispatch(
         pack(tokens), pack(cotangent), choice, scale_out, model_width, experts, splits
     )
     slot_rows = slot_rows.reshape(slot_count, model_width)
@@ -435,11 +499,11 @@
     route_out = jnp.pad(route_part.reshape(experts, 1, capacity), ((0, 0), (0, 0), (0, lane_pad)))
     back_rows, back_route, peer_squares = combine(
         token_term.astype(bf16).reshape(experts, capacity, model_width),
-        route_out, squares, experts, splits,
+        route_out, squares, got_choice, experts, splits,
     )
     squares = squares + jnp.sum(peer_squares, axis=0)
     token_grad = jnp.dot(
-        select, back_rows.reshape(slot_count, width), preferred_element_type=f32
+        group_select, back_rows.reshape(GROUPS * group_cap, width), preferred_element_type=f32
     ).astype(bf16)
     slot_route = back_route[:, 0, :capacity].reshape(1, slot_count)
     route_grad = jnp.concatenate(

time: 131 us -> 130 us (level); the launches traced: 128 us -> 129 us
  Pallas kernels: 94.1 us -> 95.7 us
    pallas_call x1, Pallas kernels: 39.2 us -> 40.7 us  [combine(): pl.pallas_call(functools.partial(combine_kernel, experts, splits), out_sh...]
where the time goes in v3:
time: 130 us; the launch traced here: 129 us
  Pallas kernels  95.7 us (74%)
  matrix products  20.6 us (16%)
  local copies, waits for them, and re-layouts  7.95 us (6%)
  other arithmetic  4.38 us (3%)
    pallas_call x1, Pallas kernels, dispatch(): pl.pallas_call(functools.partial(dispatch_kernel, experts, splits), out_s...  55 us
    pallas_call x1, Pallas kernels, combine(): pl.pallas_call(functools.partial(combine_kernel, experts, splits), out_sh...  40.7 us
    dot_general x3, matrix products, outer(): lax.dot_general(left, right, (((0,), (0,)), ((), ())), preferred_element_...  7.02 us
    unnamed x20, local copies, waits for them, and re-layouts  4.2 us

profile of v3, /device:TPU:0, one launch (start us, length us, event | category | flops | bytes accessed | tf_op | source)
XLA Modules:
  0.0 129.5 jit_solution(10374724668587481017)
XLA Ops:
  0.7 0.8 bitcast_convert_fusion.1
  1.5 0.8 slice_bitcast_fusion.5
  4.2 0.6 pad_maximum_fusion.choice_ref
  4.9 1.3 convolution_convert_fusion.3
  6.2 1.3 convolution_convert_fusion.4
  7.5 55.0 %shard_map.134 = (bf16[16,32,2048]{2,1,0:T(8,128)(2,1)}, bf16[16,32,2048]{2,1,0:T(8,128)(2,1)}, f32[16,1,128]{2,1,0:T(1,128)}, bf16[4,64,128]{2,1,0:T(8,128)(2,1)}) custom-call(bf16[4,64,1280]{2,1,0:T(8,128)(2,1)} %bitcast.74, bf16[4,64,1280]{2,1,0:T(8,128)(2,1)} %bitcast.73, bf16[4,64,128]{2,1,0:T(8,128)(2,1)} %pad_maximum_fusion.choice_ref, ...), custom_call_target="tpu_custom_call" | custom-call | tf_op jit(solution)/shard_map/pallas_call | solution.py:195
  62.5 0.8 slice_reduce_fusion.1
  63.4 2.5 %fusion.5 = f32[512,256]{0,1:T(8,128)S(1)} fusion(bf16[512,2048]{1,0:T(8,128)(2,1)} %bitcast.85, bf16[1,2048,256]{2,1,0:T(8,128)(2,1)S(1)} %copy-done), kind=kOutput, calls=%fused_computation.20 | convolution fusion | flops 536870912 | bytes 3670016 | tf_op jit(solution)/shard_map/dot_general | solution.py:467
  65.9 0.8 fusion.8
  66.7 0.8 copy-done.7
  67.8 1.7 %multiply_reduce_fusion.3 = (f32[512]{0:T(512)S(1)}, bf16[512,256]{0,1:T(8,128)(2,1)S(1)}, bf16[512,256]{0,1:T(8,128)(2,1)}) fusion(f32[512,256]{0,1:T(8,128)S(1)} %fusion.8, f32[512,256]{0,1:T(8,128)S(1)} %fusion.5, f32[512]{0:T(512)S(1)} %mul.52, bf16[512,2048]{1,0:T(8,128)(2,1)S(1)} %bitcast.89, bf16[1,256,2048]{2,1,0:T(8,128)(2,1)S(1)} %copy-done.8), kind=kOutput, calls=%fused_computation.28 | convolution fusion | flops 539098624 | bytes 4722688 | tf_op jit(solution)/shard_map/dot_general | solution.py:469
  69.4 2.3 %multiply_reduce_fusion = (f32[256]{0:T(256)}, bf16[256,2048]{1,0:T(8,128)(2,1)}) fusion(bf16[512,2048]{1,0:T(8,128)(2,1)S(1)} %bitcast.90, f32[512]{0:T(512)S(1)} %mul.52, f32[512,256]{0,1:T(8,128)S(1)} %fusion.8, f32[512,256]{0,1:T(8,128)S(1)} %fusion.5), kind=kOutput, calls=%fused_computation.6 | convolution fusion | flops 539885312 | bytes 4197376 | tf_op jit(solution)/shard_map/dot_general | solution.py:482
  72.4 2.3 %multiply_reduce_fusion.2 = (f32[2048]{0:T(1024)S(1)}, bf16[2048,256]{0,1:T(8,128)(2,1)S(1)}) fusion(bf16[512,256]{0,1:T(8,128)(2,1)S(1)} %get-tuple-element.33, bf16[512,2048]{1,0:T(8,128)(2,1)} %bitcast.86), kind=kOutput, calls=%fused_computation.8 | convolution fusion | flops 538966016 | bytes 3416064 | tf_op jit(solution)/shard_map/dot_general | solution.py:482
  74.7 2.4 %multiply_reduce_fusion.1 = (f32[2048]{0:T(1024)S(1)}, bf16[2048,256]{0,1:T(8,128)(2,1)S(1)}) fusion(bf16[512,256]{0,1:T(8,128)(2,1)} %get-tuple-element.34, bf16[512,2048]{1,0:T(8,128)(2,1)} %bitcast.87), kind=kOutput, calls=%fused_computation.7 | convolution fusion | flops 538966016 | bytes 3416064 | tf_op jit(solution)/shard_map/dot_general | solution.py:482
  77.2 1.3 %copy.16 = bf16[1,2048,256]{2,1,0:T(8,128)(2,1)} copy(bf16[1,2048,256]{1,2,0:T(8,128)(2,1)S(1)} %bitcast.76) | data formatting | bytes 2097152
  78.5 1.3 %copy.15 = bf16[1,2048,256]{2,1,0:T(8,128)(2,1)} copy(bf16[1,2048,256]{1,2,0:T(8,128)(2,1)S(1)} %bitcast.75) | data formatting | bytes 2097152
  79.8 0.6 pad_maximum_fusion.1.square_ref
  80.4 0.8 fusion.3
  81.7 2.2 %add_convert_fusion = bf16[512,2048]{1,0:T(8,128)(2,1)} fusion(f32[512,2048]{1,0:T(8,128)S(1)} %fusion.3, bf16[512,256]{0,1:T(8,128)(2,1)S(1)} %copy-done.5, bf16[1,2048,256]{2,1,0:T(8,128)(2,1)S(1)} %copy-done.2), kind=kOutput, calls=%fused_computation | convolution fusion | flops 538968064 | bytes 7602176 | tf_op jit(solution)/shard_map/dot_general | solution.py:492
  83.8 40.7 %shard_map.135 = (bf16[4,64,1024]{2,1,0:T(8,128)(2,1)}, f32[16,1,128]{2,1,0:T(1,128)}, f32[1,2,2048]{2,1,0:T(2,128)}) custom-call(bf16[16,32,2048]{2,1,0:T(8,128)(2,1)} %bitcast.72, f32[16,1,128]{2,1,0:T(1,128)} %pad.8.route_ref, f32[2,2048]{1,0:T(2,128)} %pad_maximum_fusion.1.square_ref, bf16[4,64,128]{2,1,0:T(8,128)(2,1)} %get-tuple-element.18.choice_ref), custom_call_target="tpu_custom_call" | custom-call | tf_op jit(solution)/shard_map/pallas_call | solution.py:363
  124.5 0.7 bitcast_add_fusion
  125.3 2.0 %convolution_convert_fusion.6 = bf16[128,1024]{1,0:T(8,128)(2,1)} fusion(bf16[256,1024]{1,0:T(8,128)(2,1)} %bitcast.77, s32[128]{0:T(128)S(1)} %fusion.52), kind=kOutput, calls=%fused_computation.10 | convolution fusion | flops 67272704 | bytes 786944 | tf_op jit(solution)/shard_map/dot_general | solution.py:505
  127.3 0.6 fusion.59
  127.9 0.7 slice_reduce_fusion
  (37 shorter events, 4.3 us)
Async XLA Ops:
  0.6 62.7 %copy-start = (bf16[1,2048,256]{2,1,0:T(8,128)(2,1)S(1)}, bf16[1,2048,256]{2,1,0:T(8,128)(2,1)}, u32[]{:S(2)}) copy-start(bf16[1,2048,256]{2,1,0:T(8,128)(2,1)} %param.11) | copy-start | bytes 3145732
  0.6 4.2 %copy-start.4 = (bf16[128,2048]{1,0:T(8,128)(2,1)S(1)}, bf16[128,2048]{1,0:T(8,128)(2,1)}, u32[]{:S(2)}) copy-start(bf16[128,2048]{1,0:T(8,128)(2,1)} %param.10) | copy-start | bytes 1572868
  0.7 4.2 %slice-start.1 = ((bf16[128,2048]{1,0:T(8,128)(2,1)}), bf16[128,512]{1,0:T(8,128)(2,1)S(1)}, s32[]{:S(2)}) async-start(bf16[128,2048]{1,0:T(8,128)(2,1)} %param.10), calls=%async_computation.1 | async-start | bytes 262144 | tf_op jit(solution)/shard_map/slice | solution.py:448
  0.7 4.2 %copy-start.3 = (bf16[128,2048]{1,0:T(8,128)(2,1)S(1)}, bf16[128,2048]{1,0:T(8,128)(2,1)}, u32[]{:S(2)}) copy-start(bf16[128,2048]{1,0:T(8,128)(2,1)} %param.7) | copy-start | bytes 1572868
  0.7 5.5 %slice-start = ((bf16[128,2048]{1,0:T(8,128)(2,1)}), bf16[128,512]{1,0:T(8,128)(2,1)S(1)}, s32[]{:S(2)}) async-start(bf16[128,2048]{1,0:T(8,128)(2,1)} %param.7), calls=%async_computation | async-start | bytes 262144 | tf_op jit(solution)/shard_map/slice | solution.py:448
  62.5 3.4 %copy-start.1 = (bf16[1,2048,256]{2,1,0:T(8,128)(2,1)S(1)}, bf16[1,2048,256]{2,1,0:T(8,128)(2,1)}, u32[]{:S(2)}) copy-start(bf16[1,2048,256]{2,1,0:T(8,128)(2,1)} %param.12) | copy-start | bytes 3145732
  63.4 2.5 %copy-start.6 = (bf16[16,32,2048]{2,1,0:T(8,128)(2,1)S(1)}, bf16[16,32,2048]{2,1,0:T(8,128)(2,1)}, u32[]{:S(2)}) copy-start(bf16[16,32,2048]{2,1,0:T(8,128)(2,1)} %get-tuple-element.17) | copy-start | bytes 6291460
  65.9 1.6 %copy-start.7 = (bf16[16,32,2048]{2,1,0:T(8,128)(2,1)S(1)}, bf16[16,32,2048]{2,1,0:T(8,128)(2,1)}, u32[]{:S(2)}) copy-start(bf16[16,32,2048]{2,1,0:T(8,128)(2,1)} %get-tuple-element.16) | copy-start | bytes 6291460
  65.9 1.8 %copy-start.8 = (bf16[1,256,2048]{2,1,0:T(8,128)(2,1)S(1)}, bf16[1,256,2048]{2,1,0:T(8,128)(2,1)}, u32[]{:S(2)}) copy-start(bf16[1,256,2048]{2,1,0:T(8,128)(2,1)} %param.13) | copy-start | bytes 3145732
  80.4 1.2 copy-start.2
  80.4 1.3 copy-start.5

commit v4 on v3

--- a/solution.py
+++ b/solution.py
@@ -9,7 +9,7 @@
 
 MESH = pl.DeviceIdType.MESH
 LANES = 128
-SHARE = 4
+SHARE = 3
 GROUPS = 4
 
 
@@ -132,11 +132,12 @@
             def _(hop):
                 near_copy(step, hop, i).start()
 
-            if shared:
-
-                @pl.loop(1, members)
-                def _(hop):
-                    near_copy(step, hop, i + 2).start()
+        if shared:
+
+            @pl.loop(1, members)
+            def _(hop):
+                for n in range(2, len(views)):
+                    near_copy(step, hop, n).start()
 
         if step == 0:
 
@@ -439,7 +440,7 @@
         ]
     )
     width = model_width // splits
-    shared = model_width // SHARE // (splits * LANES) * (splits * LANES) if SHARE else 0
+    shared = model_width * SHARE // 8 // (splits * LANES) * (splits * LANES)
     cut = (model_width - shared) // splits
     start = lax.axis_index("tp") * cut
 

time: 130 us -> 130 us (level)
  no operation moved by 1% of the time
where the time goes in v4:
time: 130 us
  Pallas kernels  96.1 us (74%)
  matrix products  20.7 us (16%)
  local copies, waits for them, and re-layouts  7.96 us (6%)
  other arithmetic  4.38 us (3%)
    pallas_call x1, Pallas kernels, dispatch(): pl.pallas_call(functools.partial(dispatch_kernel, experts, splits), out_s...  54.4 us
    pallas_call x1, Pallas kernels, combine(): pl.pallas_call(functools.partial(combine_kernel, experts, splits), out_sh...  41.7 us
    dot_general x3, matrix products, outer(): lax.dot_general(left, right, (((0,), (0,)), ((), ())), preferred_element_...  7.02 us
    unnamed x20, local copies, waits for them, and re-layouts  4.2 us
    dot_general x2, matrix products, pack(): lax.dot_general(group_select, piece, (((0,), (0,)), ((), ())), preferred_...  2.65 us

profile of v4, /device:TPU:0, one launch (start us, length us, event | category | flops | bytes accessed | tf_op | source)
XLA Modules:
  0.0 130.0 jit_solution(12418861315164583350)
XLA Ops:
  0.7 0.8 bitcast_convert_fusion.1
  1.5 0.8 slice_bitcast_fusion.5
  4.2 0.6 pad_maximum_fusion.choice_ref
  4.9 1.3 %convolution_convert_fusion.3 = bf16[256,1408]{1,0:T(8,128)(2,1)} fusion(bf16[128,768]{1,0:T(8,128)(2,1)S(1)} %slice-done.1, bf16[128,640]{1,0:T(8,128)(2,1)S(1)} %get-tuple-element.52, s32[128]{0:T(128)S(1)} %fusion.52), kind=kOutput, calls=%fused_computation.4 | convolution fusion | flops 93388800 | bytes 1081856 | tf_op jit(solution)/shard_map/dot_general | solution.py:451
  6.2 1.3 %convolution_convert_fusion.4 = bf16[256,1408]{1,0:T(8,128)(2,1)} fusion(bf16[128,768]{1,0:T(8,128)(2,1)S(1)} %slice-done, bf16[128,640]{1,0:T(8,128)(2,1)S(1)} %get-tuple-element.53, s32[128]{0:T(128)S(1)} %fusion.52), kind=kOutput, calls=%fused_computation.5 | convolution fusion | flops 93388800 | bytes 1081856 | tf_op jit(solution)/shard_map/dot_general | solution.py:451
  7.6 54.4 %shard_map.134 = (bf16[16,32,2048]{2,1,0:T(8,128)(2,1)}, bf16[16,32,2048]{2,1,0:T(8,128)(2,1)}, f32[16,1,128]{2,1,0:T(1,128)}, bf16[4,64,128]{2,1,0:T(8,128)(2,1)}) custom-call(bf16[4,64,1408]{2,1,0:T(8,128)(2,1)} %bitcast.74, bf16[4,64,1408]{2,1,0:T(8,128)(2,1)} %bitcast.73, bf16[4,64,128]{2,1,0:T(8,128)(2,1)} %pad_maximum_fusion.choice_ref, ...), custom_call_target="tpu_custom_call" | custom-call | tf_op jit(solution)/shard_map/pallas_call | solution.py:196
  62.0 0.8 slice_reduce_fusion.1
  62.9 2.5 %fusion.5 = f32[512,256]{0,1:T(8,128)S(1)} fusion(bf16[512,2048]{1,0:T(8,128)(2,1)} %bitcast.85, bf16[1,2048,256]{2,1,0:T(8,128)(2,1)S(1)} %copy-done), kind=kOutput, calls=%fused_computation.20 | convolution fusion | flops 536870912 | bytes 3670016 | tf_op jit(solution)/shard_map/dot_general | solution.py:468
  65.4 0.8 fusion.8
  66.2 0.8 copy-done.7
  67.2 1.7 %multiply_reduce_fusion.3 = (f32[512]{0:T(512)S(1)}, bf16[512,256]{0,1:T(8,128)(2,1)S(1)}, bf16[512,256]{0,1:T(8,128)(2,1)}) fusion(f32[512,256]{0,1:T(8,128)S(1)} %fusion.8, f32[512,256]{0,1:T(8,128)S(1)} %fusion.5, f32[512]{0:T(512)S(1)} %mul.52, bf16[512,2048]{1,0:T(8,128)(2,1)S(1)} %bitcast.89, bf16[1,256,2048]{2,1,0:T(8,128)(2,1)S(1)} %copy-done.8), kind=kOutput, calls=%fused_computation.28 | convolution fusion | flops 539098624 | bytes 4722688 | tf_op jit(solution)/shard_map/dot_general | solution.py:470
  68.9 2.3 %multiply_reduce_fusion = (f32[256]{0:T(256)}, bf16[256,2048]{1,0:T(8,128)(2,1)}) fusion(bf16[512,2048]{1,0:T(8,128)(2,1)S(1)} %bitcast.90, f32[512]{0:T(512)S(1)} %mul.52, f32[512,256]{0,1:T(8,128)S(1)} %fusion.8, f32[512,256]{0,1:T(8,128)S(1)} %fusion.5), kind=kOutput, calls=%fused_computation.6 | convolution fusion | flops 539885312 | bytes 4197376 | tf_op jit(solution)/shard_map/dot_general | solution.py:483
  71.9 2.3 %multiply_reduce_fusion.2 = (f32[2048]{0:T(1024)S(1)}, bf16[2048,256]{0,1:T(8,128)(2,1)S(1)}) fusion(bf16[512,256]{0,1:T(8,128)(2,1)S(1)} %get-tuple-element.33, bf16[512,2048]{1,0:T(8,128)(2,1)} %bitcast.86), kind=kOutput, calls=%fused_computation.8 | convolution fusion | flops 538966016 | bytes 3416064 | tf_op jit(solution)/shard_map/dot_general | solution.py:483
  74.2 2.4 %multiply_reduce_fusion.1 = (f32[2048]{0:T(1024)S(1)}, bf16[2048,256]{0,1:T(8,128)(2,1)S(1)}) fusion(bf16[512,256]{0,1:T(8,128)(2,1)} %get-tuple-element.34, bf16[512,2048]{1,0:T(8,128)(2,1)} %bitcast.87), kind=kOutput, calls=%fused_computation.7 | convolution fusion | flops 538966016 | bytes 3416064 | tf_op jit(solution)/shard_map/dot_general | solution.py:483
  76.6 1.3 %copy.16 = bf16[1,2048,256]{2,1,0:T(8,128)(2,1)} copy(bf16[1,2048,256]{1,2,0:T(8,128)(2,1)S(1)} %bitcast.76) | data formatting | bytes 2097152
  77.9 1.3 copy.15
  79.2 0.6 pad_maximum_fusion.1.square_ref
  79.9 0.8 fusion.3
  81.1 2.2 %add_convert_fusion = bf16[512,2048]{1,0:T(8,128)(2,1)} fusion(f32[512,2048]{1,0:T(8,128)S(1)} %fusion.3, bf16[512,256]{0,1:T(8,128)(2,1)S(1)} %copy-done.5, bf16[1,2048,256]{2,1,0:T(8,128)(2,1)S(1)} %copy-done.2), kind=kOutput, calls=%fused_computation | convolution fusion | flops 538968064 | bytes 7602176 | tf_op jit(solution)/shard_map/dot_general | solution.py:493
  83.3 41.7 %shard_map.135 = (bf16[4,64,1024]{2,1,0:T(8,128)(2,1)}, f32[16,1,128]{2,1,0:T(1,128)}, f32[1,2,2048]{2,1,0:T(2,128)}) custom-call(bf16[16,32,2048]{2,1,0:T(8,128)(2,1)} %bitcast.72, f32[16,1,128]{2,1,0:T(1,128)} %pad.8.route_ref, f32[2,2048]{1,0:T(2,128)} %pad_maximum_fusion.1.square_ref, bf16[4,64,128]{2,1,0:T(8,128)(2,1)} %get-tuple-element.18.choice_ref), custom_call_target="tpu_custom_call" | custom-call | tf_op jit(solution)/shard_map/pallas_call | solution.py:364
  125.0 0.7 bitcast_add_fusion
  125.8 2.0 %convolution_convert_fusion.6 = bf16[128,1024]{1,0:T(8,128)(2,1)} fusion(bf16[256,1024]{1,0:T(8,128)(2,1)} %bitcast.77, s32[128]{0:T(128)S(1)} %fusion.52), kind=kOutput, calls=%fused_computation.10 | convolution fusion | flops 67272704 | bytes 786944 | tf_op jit(solution)/shard_map/dot_general | solution.py:506
  127.8 0.6 fusion.59
  128.4 0.7 slice_reduce_fusion
  (37 shorter events, 4.3 us)
Async XLA Ops:
  0.6 62.2 %copy-start = (bf16[1,2048,256]{2,1,0:T(8,128)(2,1)S(1)}, bf16[1,2048,256]{2,1,0:T(8,128)(2,1)}, u32[]{:S(2)}) copy-start(bf16[1,2048,256]{2,1,0:T(8,128)(2,1)} %param.11) | copy-start | bytes 3145732
  0.6 4.2 %copy-start.4 = (bf16[128,2048]{1,0:T(8,128)(2,1)S(1)}, bf16[128,2048]{1,0:T(8,128)(2,1)}, u32[]{:S(2)}) copy-start(bf16[128,2048]{1,0:T(8,128)(2,1)} %param.10) | copy-start | bytes 1572868
  0.7 4.2 %slice-start.1 = ((bf16[128,2048]{1,0:T(8,128)(2,1)}), bf16[128,768]{1,0:T(8,128)(2,1)S(1)}, s32[]{:S(2)}) async-start(bf16[128,2048]{1,0:T(8,128)(2,1)} %param.10), calls=%async_computation.1 | async-start | bytes 393216 | tf_op jit(solution)/shard_map/slice | solution.py:449
  0.7 4.2 %copy-start.3 = (bf16[128,2048]{1,0:T(8,128)(2,1)S(1)}, bf16[128,2048]{1,0:T(8,128)(2,1)}, u32[]{:S(2)}) copy-start(bf16[128,2048]{1,0:T(8,128)(2,1)} %param.7) | copy-start | bytes 1572868
  2.5 3.8 %slice-start = ((bf16[128,2048]{1,0:T(8,128)(2,1)}), bf16[128,768]{1,0:T(8,128)(2,1)S(1)}, s32[]{:S(2)}) async-start(bf16[128,2048]{1,0:T(8,128)(2,1)} %param.7), calls=%async_computation | async-start | bytes 393216 | tf_op jit(solution)/shard_map/slice | solution.py:449
  61.9 3.4 %copy-start.1 = (bf16[1,2048,256]{2,1,0:T(8,128)(2,1)S(1)}, bf16[1,2048,256]{2,1,0:T(8,128)(2,1)}, u32[]{:S(2)}) copy-start(bf16[1,2048,256]{2,1,0:T(8,128)(2,1)} %param.12) | copy-start | bytes 3145732
  62.9 2.5 %copy-start.6 = (bf16[16,32,2048]{2,1,0:T(8,128)(2,1)S(1)}, bf16[16,32,2048]{2,1,0:T(8,128)(2,1)}, u32[]{:S(2)}) copy-start(bf16[16,32,2048]{2,1,0:T(8,128)(2,1)} %get-tuple-element.17) | copy-start | bytes 6291460
  65.4 1.6 %copy-start.7 = (bf16[16,32,2048]{2,1,0:T(8,128)(2,1)S(1)}, bf16[16,32,2048]{2,1,0:T(8,128)(2,1)}, u32[]{:S(2)}) copy-start(bf16[16,32,2048]{2,1,0:T(8,128)(2,1)} %get-tuple-element.16) | copy-start | bytes 6291460
  65.4 1.8 %copy-start.8 = (bf16[1,256,2048]{2,1,0:T(8,128)(2,1)S(1)}, bf16[1,256,2048]{2,1,0:T(8,128)(2,1)}, u32[]{:S(2)}) copy-start(bf16[1,256,2048]{2,1,0:T(8,128)(2,1)} %param.13) | copy-start | bytes 3145732
  79.9 1.2 copy-start.2
  79.9 1.3 copy-start.5

commit v5 on v3

--- a/solution.py
+++ b/solution.py
@@ -4,6 +4,7 @@
 import jax.numpy as jnp
 from jax import lax
 from jax.experimental import pallas as pl
+from jax.experimental.layout import Layout, with_layout_constraint
 from jax.experimental.pallas import tpu as pltpu
 from jax.sharding import PartitionSpec as P
 
@@ -484,8 +485,9 @@
         ).astype(bf16)
 
     grad_down = outer(weighted_hidden, slot_cot)
-    grad_gate = outer(slot_rows, gate_cot)
-    grad_up = outer(slot_rows, up_cot)
+    by_rows = Layout(major_to_minor=(0, 1))
+    grad_gate = with_layout_constraint(outer(slot_rows, gate_cot), by_rows)
+    grad_up = with_layout_constraint(outer(slot_rows, up_cot), by_rows)
     token_term = lax.dot_general(
         gate_cot, gate_cols, (((1,), (1,)), ((), ())), preferred_element_type=f32
     )

time: 130 us -> 127 us (0.977)
  local copies, waits for them, and re-layouts: 7.95 us -> 4.85 us
    unnamed x20 -> x16, local copies, waits for them, and re-layouts: 4.2 us -> 1.1 us
where the time goes in v5:
time: 127 us; the launch traced here: 126 us
  Pallas kernels  95.7 us (75%)
  matrix products  20.6 us (16%)
  local copies, waits for them, and re-layouts  4.85 us (4%)
  other arithmetic  4.39 us (3%)
    pallas_call x1, Pallas kernels, dispatch(): pl.pallas_call(functools.partial(dispatch_kernel, experts, splits), out_s...  55 us
    pallas_call x1, Pallas kernels, combine(): pl.pallas_call(functools.partial(combine_kernel, experts, splits), out_sh...  40.7 us
    dot_general x3, matrix products, outer(): lax.dot_general(left, right, (((0,), (0,)), ((), ())), preferred_element_...  7.7 us
    dot_general x2, matrix products, pack(): lax.dot_general(group_select, piece, (((0,), (0,)), ((), ())), preferred_...  2.57 us

profile of v5, /device:TPU:0, one launch (start us, length us, event | category | flops | bytes accessed | tf_op | source)
XLA Modules:
  0.0 126.4 jit_solution(13056355829028642269)
XLA Ops:
  0.7 0.8 bitcast_convert_fusion.1
  1.5 0.8 slice_bitcast_fusion.5
  3.2 0.6 pad.7.scale_ref
  4.2 0.6 pad_maximum_fusion.choice_ref
  4.9 1.3 %convolution_convert_fusion.3 = bf16[256,1280]{1,0:T(8,128)(2,1)} fusion(bf16[128,512]{1,0:T(8,128)(2,1)S(1)} %slice-done.1, bf16[128,768]{1,0:T(8,128)(2,1)S(1)} %get-tuple-element.44, s32[128]{0:T(128)S(1)} %fusion.52), kind=kOutput, calls=%fused_computation.4 | convolution fusion | flops 84901888 | bytes 983552 | tf_op jit(solution)/shard_map/dot_general | solution.py:451
  6.2 1.3 %convolution_convert_fusion.4 = bf16[256,1280]{1,0:T(8,128)(2,1)} fusion(bf16[128,512]{1,0:T(8,128)(2,1)S(1)} %slice-done, bf16[128,768]{1,0:T(8,128)(2,1)S(1)} %get-tuple-element.45, s32[128]{0:T(128)S(1)} %fusion.52), kind=kOutput, calls=%fused_computation.5 | convolution fusion | flops 84901888 | bytes 983552 | tf_op jit(solution)/shard_map/dot_general | solution.py:451
  7.5 55.0 %shard_map.134 = (bf16[16,32,2048]{2,1,0:T(8,128)(2,1)}, bf16[16,32,2048]{2,1,0:T(8,128)(2,1)}, f32[16,1,128]{2,1,0:T(1,128)}, bf16[4,64,128]{2,1,0:T(8,128)(2,1)}) custom-call(bf16[4,64,1280]{2,1,0:T(8,128)(2,1)} %bitcast.74, bf16[4,64,1280]{2,1,0:T(8,128)(2,1)} %bitcast.73, bf16[4,64,128]{2,1,0:T(8,128)(2,1)} %pad_maximum_fusion.choice_ref, ...), custom_call_target="tpu_custom_call" | custom-call | tf_op jit(solution)/shard_map/pallas_call | solution.py:196
  62.5 0.8 slice_reduce_fusion.1
  63.4 2.5 %fusion.5 = f32[512,256]{0,1:T(8,128)S(1)} fusion(bf16[512,2048]{1,0:T(8,128)(2,1)} %bitcast.83, bf16[1,2048,256]{2,1,0:T(8,128)(2,1)S(1)} %copy-done), kind=kOutput, calls=%fused_computation.20 | convolution fusion | flops 536870912 | bytes 3670016 | tf_op jit(solution)/shard_map/dot_general | solution.py:468
  65.9 0.8 fusion.8
  66.7 0.8 copy-done.6
  67.8 1.0 multiply_reduce_fusion.3
  68.7 2.3 %multiply_reduce_fusion = (f32[256]{0:T(256)}, bf16[256,2048]{1,0:T(8,128)(2,1)}) fusion(bf16[512,2048]{1,0:T(8,128)(2,1)S(1)} %bitcast.88, f32[512]{0:T(512)S(1)} %mul.52, f32[512,256]{0,1:T(8,128)S(1)} %fusion.8, f32[512,256]{0,1:T(8,128)S(1)} %fusion.5), kind=kOutput, calls=%fused_computation.6 | convolution fusion | flops 539885312 | bytes 4197376 | tf_op jit(solution)/shard_map/dot_general | solution.py:483
  71.1 0.6 pad.8.route_ref
  71.7 3.6 %multiply_reduce_fusion.2 = (f32[2048]{0:T(1024)S(1)}, bf16[2048,256]{1,0:T(8,128)(2,1)}) fusion(bf16[512,2048]{1,0:T(8,128)(2,1)} %bitcast.84, bf16[512,256]{0,1:T(8,128)(2,1)S(1)} %get-tuple-element.25), kind=kOutput, calls=%fused_computation.8 | convolution fusion | flops 538966016 | bytes 3416064 | tf_op jit(solution)/shard_map/dot_general | solution.py:483
  75.3 1.8 %multiply_reduce_fusion.1 = (f32[2048]{0:T(1024)S(1)}, bf16[2048,256]{1,0:T(8,128)(2,1)}) fusion(bf16[512,2048]{1,0:T(8,128)(2,1)S(1)} %bitcast.86, bf16[512,256]{0,1:T(8,128)(2,1)S(1)} %get-tuple-element.26), kind=kOutput, calls=%fused_computation.7 | convolution fusion | flops 538966016 | bytes 3416064 | tf_op jit(solution)/shard_map/dot_general | solution.py:483
  77.1 0.6 pad_maximum_fusion.1.square_ref
  77.7 0.8 fusion.3
  78.5 2.2 %add_convert_fusion = bf16[512,2048]{1,0:T(8,128)(2,1)} fusion(f32[512,2048]{1,0:T(8,128)S(1)} %fusion.3, bf16[512,256]{0,1:T(8,128)(2,1)S(1)} %get-tuple-element.26, bf16[1,2048,256]{2,1,0:T(8,128)(2,1)S(1)} %copy-done.1), kind=kOutput, calls=%fused_computation | convolution fusion | flops 538968064 | bytes 7602176 | tf_op jit(solution)/shard_map/dot_general | solution.py:494
  80.7 40.7 %shard_map.135 = (bf16[4,64,1024]{2,1,0:T(8,128)(2,1)}, f32[16,1,128]{2,1,0:T(1,128)}, f32[1,2,2048]{2,1,0:T(2,128)}) custom-call(bf16[16,32,2048]{2,1,0:T(8,128)(2,1)} %bitcast.72, f32[16,1,128]{2,1,0:T(1,128)} %pad.8.route_ref, f32[2,2048]{1,0:T(2,128)} %pad_maximum_fusion.1.square_ref, bf16[4,64,128]{2,1,0:T(8,128)(2,1)} %get-tuple-element.18.choice_ref), custom_call_target="tpu_custom_call" | custom-call | tf_op jit(solution)/shard_map/pallas_call | solution.py:364
  121.4 0.7 bitcast_add_fusion
  122.1 2.0 %convolution_convert_fusion.6 = bf16[128,1024]{1,0:T(8,128)(2,1)} fusion(bf16[256,1024]{1,0:T(8,128)(2,1)} %bitcast.75, s32[128]{0:T(128)S(1)} %fusion.52), kind=kOutput, calls=%fused_computation.10 | convolution fusion | flops 67272704 | bytes 786944 | tf_op jit(solution)/shard_map/dot_general | solution.py:507
  124.2 0.6 fusion.59
  124.8 0.7 slice_reduce_fusion
  (33 shorter events, 2.6 us)
Async XLA Ops:
  0.6 62.7 %copy-start = (bf16[1,2048,256]{2,1,0:T(8,128)(2,1)S(1)}, bf16[1,2048,256]{2,1,0:T(8,128)(2,1)}, u32[]{:S(2)}) copy-start(bf16[1,2048,256]{2,1,0:T(8,128)(2,1)} %param.11) | copy-start | bytes 3145732
  0.6 4.2 %copy-start.3 = (bf16[128,2048]{1,0:T(8,128)(2,1)S(1)}, bf16[128,2048]{1,0:T(8,128)(2,1)}, u32[]{:S(2)}) copy-start(bf16[128,2048]{1,0:T(8,128)(2,1)} %param.10) | copy-start | bytes 1572868
  0.7 4.2 %slice-start.1 = ((bf16[128,2048]{1,0:T(8,128)(2,1)}), bf16[128,512]{1,0:T(8,128)(2,1)S(1)}, s32[]{:S(2)}) async-start(bf16[128,2048]{1,0:T(8,128)(2,1)} %param.10), calls=%async_computation.1 | async-start | bytes 262144 | tf_op jit(solution)/shard_map/slice | solution.py:449
  0.7 4.2 %copy-start.2 = (bf16[128,2048]{1,0:T(8,128)(2,1)S(1)}, bf16[128,2048]{1,0:T(8,128)(2,1)}, u32[]{:S(2)}) copy-start(bf16[128,2048]{1,0:T(8,128)(2,1)} %param.7) | copy-start | bytes 1572868
  0.7 5.5 %slice-start = ((bf16[128,2048]{1,0:T(8,128)(2,1)}), bf16[128,512]{1,0:T(8,128)(2,1)S(1)}, s32[]{:S(2)}) async-start(bf16[128,2048]{1,0:T(8,128)(2,1)} %param.7), calls=%async_computation | async-start | bytes 262144 | tf_op jit(solution)/shard_map/slice | solution.py:449
  62.5 3.4 %copy-start.1 = (bf16[1,2048,256]{2,1,0:T(8,128)(2,1)S(1)}, bf16[1,2048,256]{2,1,0:T(8,128)(2,1)}, u32[]{:S(2)}) copy-start(bf16[1,2048,256]{2,1,0:T(8,128)(2,1)} %param.12) | copy-start | bytes 3145732
  63.4 2.5 %copy-start.4 = (bf16[16,32,2048]{2,1,0:T(8,128)(2,1)S(1)}, bf16[16,32,2048]{2,1,0:T(8,128)(2,1)}, u32[]{:S(2)}) copy-start(bf16[16,32,2048]{2,1,0:T(8,128)(2,1)} %get-tuple-element.17) | copy-start | bytes 6291460
  65.9 1.6 %copy-start.6 = (bf16[16,32,2048]{2,1,0:T(8,128)(2,1)S(1)}, bf16[16,32,2048]{2,1,0:T(8,128)(2,1)}, u32[]{:S(2)}) copy-start(bf16[16,32,2048]{2,1,0:T(8,128)(2,1)} %get-tuple-element.16) | copy-start | bytes 6291460
  65.9 1.8 %copy-start.7 = (bf16[1,256,2048]{2,1,0:T(8,128)(2,1)S(1)}, bf16[1,256,2048]{2,1,0:T(8,128)(2,1)}, u32[]{:S(2)}) copy-start(bf16[1,256,2048]{2,1,0:T(8,128)(2,1)} %param.13) | copy-start | bytes 3145732
  71.7 3.6 %copy-start.5 = (bf16[16,32,2048]{2,1,0:T(8,128)(2,1)S(1)}, bf16[16,32,2048]{2,1,0:T(8,128)(2,1)}, u32[]{:S(2)}) copy-start(bf16[16,32,2048]{2,1,0:T(8,128)(2,1)} %get-tuple-element.17) | copy-start | bytes 6291460
